TPU v7x, 512 devices: a whole 4x8x8 slice. The times are simulated.
512 devices in a mesh: sp: 128 (over z, y, core), tp: 4 (over x).
Axes of the slice: x: 4, y: 8, z: 8, core: 2. Of those that a mesh axis runs over, the one named last changes fastest.
Arguments:
- tokens: bfloat16 [65536, 2048], P('sp', 'tp'), may hold values from -6 to 6
- norm_gain: float32 [2048], replicated, may hold values from 0.1 to 1.9
- query_weight: bfloat16 [2048, 2048], P('sp', 'tp'), may hold values from -0.125 to 0.125
- key_weight: bfloat16 [2048, 512], P('sp', 'tp'), may hold values from -0.125 to 0.125
- value_weight: bfloat16 [2048, 512], P('sp', 'tp'), may hold values from -0.125 to 0.125
- pool_in_weight: bfloat16 [2048, 1024], P('sp', 'tp'), may hold values from -0.125 to 0.125
- pool_mix_weight: bfloat16 [4, 256, 256], P('tp'), may hold values from -0.375 to 0.375
- sink_logit: float32 [32], P('tp'), may hold values from -300 to 300
- out_pool_weight: bfloat16 [1024, 2048], P('tp', 'sp'), may hold values from -0.109375 to 0.109375
- out_attn_weight: bfloat16 [2048, 2048], P('tp', 'sp'), may hold values from -1.25 to 1.25
Outputs:
- mixed: bfloat16 [65536, 2048], P('sp', 'tp')
- log_weight: float32 [32, 65536], P('tp', 'sp')
All inputs are finite; a program needn't handle non-finite values.
Results may differ from a plain program's by a relative error of at most 0.012.
Values may be sent and summed in bfloat16 or wider, within the bound.
A program may use at most 64 MiB of HBM per device.

v0:
```python
import jax
import jax.numpy as jnp
from jax import lax
from jax.sharding import Mesh
from jax.sharding import PartitionSpec as P

HD = 64
WINDOW = 128
GRID_W = 64
SP = ("sp_0", "sp_1", "sp_2")


norm_eps = 1e-06
rope_base = 10000.0
pool_reach = 8
neg_fill = -1e30


def sent_to_all(shard, axis):
    count = lax.axis_size(axis)
    return lax.all_to_all(
        jnp.broadcast_to(shard[None], (count, *shard.shape)), axis, 0, 0, tiled=True
    )


def laid_out(blocks, dim):
    lengths = list(blocks.shape[1:])
    lengths[dim] *= blocks.shape[0]
    return jnp.moveaxis(blocks, 0, dim).reshape(lengths)


def gathered_by_axis(shard, axes, dim):
    far, near = axes
    first = sent_to_all(shard, far)
    blocks = jnp.swapaxes(sent_to_all(first, near), 0, 1)
    return laid_out(blocks.reshape(-1, *shard.shape), dim)


def side_by_side(arrays, axis, dim, along):
    both = jnp.concatenate(arrays, axis=along)
    out, at, gathered = (gathered_by_axis(both, axis, dim), 0, [])
    for a in arrays:
        gathered.append(lax.slice_in_dim(out, at, at + a.shape[along], axis=along))
        at += a.shape[along]
    return tuple(gathered)


def collect(shard, axis, dim):
    blocks = sent_to_all(shard, axis)
    return laid_out(blocks, dim)


def in_one_piece(arrays, axis, dim, along):
    widths = [a.shape[along] for a in arrays]
    both = jnp.concatenate(arrays, axis=along)
    out = lax.all_gather(both, axis, axis=dim, tiled=True)
    return tuple(jnp.split(out, [sum(widths[:k]) for k in range(1, len(widths))], axis=along))


def with_halo(cells, sides, width):
    for axis, dim in sides:
        count = lax.axis_size(axis)
        ends = count - 1
        head = lax.slice_in_dim(cells, 0, width, axis=dim)
        tail = lax.slice_in_dim(cells, cells.shape[dim] - width, cells.shape[dim], axis=dim)
        cells = jnp.concatenate(
            [
                lax.ppermute(tail, axis, [(i, (i + 1) % count) for i in range(ends)]),
                cells,
                lax.ppermute(head, axis, [((i + 1) % count, i) for i in range(ends)]),
            ],
            axis=dim,
        )
    return cells


def in_blocks(shard, dim, count):
    lengths = shard.shape
    blocks = shard.reshape(*lengths[:dim], count, lengths[dim] // count, *lengths[dim + 1 :])
    return jnp.moveaxis(blocks, dim, 0)


def summed_on_arrival(shard, axis, dim):
    count = lax.axis_size(axis)
    blocks = lax.all_to_all(in_blocks(shard, dim, count), axis, 0, 0, tiled=True)
    return jnp.sum(blocks.astype(jnp.float32), axis=0)


def rope_tables(positions, head_dim):
    n_freq = head_dim // 4
    freqs = rope_base ** (-jnp.arange(n_freq, dtype=jnp.float32) / n_freq)
    rows = (positions // GRID_W).astype(jnp.float32)
    columns = (positions % GRID_W).astype(jnp.float32)
    row_angle = rows[:, None] * freqs[None, :]
    col_angle = columns[:, None] * freqs[None, :]
    return (jnp.cos(row_angle), jnp.sin(row_angle), jnp.cos(col_angle), jnp.sin(col_angle))


def rotate_half(values, cosine, sine):
    middle = values.shape[-1] // 2
    first = values[..., :middle]
    second = values[..., middle:]
    return jnp.concatenate([first * cosine - second * sine, second * cosine + first * sine], -1)


def rotate_heads(values, tables, head_dim):
    rows_count = values.shape[0]
    shaped = values.astype(jnp.float32).reshape(rows_count, -1, head_dim)
    cos_r, sin_r, cos_c, sin_c = [table[:, None, :] for table in tables]
    split = head_dim // 2
    turned = jnp.concatenate(
        [
            rotate_half(shaped[..., :split], cos_r, sin_r),
            rotate_half(shaped[..., split:], cos_c, sin_c),
        ],
        -1,
    )
    return turned.reshape(rows_count, -1).astype(jnp.bfloat16)


def pool_group(extended, own, positions, half_width, seq_total):
    rows_count = own.shape[0]
    summed = jnp.zeros(own.shape, jnp.float32)
    counted = jnp.zeros((rows_count,), jnp.float32)
    for shift_by in range(-pool_reach, pool_reach):
        source = positions + shift_by
        inside = (
            (shift_by >= -half_width)
            & (shift_by < half_width)
            & (source >= 0)
            & (source < seq_total)
        )
        window_rows = extended[pool_reach + shift_by : pool_reach + shift_by + rows_count].astype(
            jnp.float32
        )
        summed = summed + jnp.where(inside[:, None], window_rows, 0.0)
        counted = counted + inside.astype(jnp.float32)
    return (summed / counted[:, None] - own.astype(jnp.float32)).astype(jnp.bfloat16)


def attend_block(queries, keys, values, sink, query_pos, key_pos, seq_total):
    scores = jnp.einsum(
        "qhgd,khd->hgqk", queries, keys, preferred_element_type=jnp.float32
    ) * HD ** (-0.5)
    valid = (
        (jnp.abs(query_pos[:, None] - key_pos[None, :]) <= WINDOW)
        & (key_pos >= 0)[None, :]
        & (key_pos < seq_total)[None, :]
    )
    scores = jnp.where(valid, scores, neg_fill)
    row_top = jnp.maximum(jnp.max(scores, -1), sink[:, :, None])
    exps = jnp.exp(scores - row_top[..., None])
    row_total = jnp.sum(exps, -1) + jnp.exp(sink[:, :, None] - row_top)
    weights = (exps / row_total[..., None]).astype(jnp.bfloat16)
    attended = jnp.einsum("hgqk,khd->qhgd", weights, values, preferred_element_type=jnp.float32)
    return (attended.astype(jnp.bfloat16), row_top + jnp.log(row_total))


def fetch_outputs(out_pool_weight, out_attn_weight):
    return side_by_side((out_pool_weight, out_attn_weight), (("sp_0", "sp_1"), "sp_2"), 1, 0)


def local(
    tokens,
    norm_gain,
    query_weight,
    key_weight,
    value_weight,
    pool_in_weight,
    pool_mix_weight,
    sink_logit,
    out_pool_weight,
    out_attn_weight,
):
    whole = collect(tokens, "tp", 1)
    wide = whole.astype(jnp.float32)
    normed = (
        wide * lax.rsqrt(jnp.mean(wide * wide, -1, keepdims=True) + norm_eps) * norm_gain
    ).astype(jnp.bfloat16)
    tok_rows = normed.shape[0]
    seq_total = tok_rows * lax.axis_size(SP)
    offset = lax.axis_index(SP) * tok_rows
    weights_in = (query_weight, key_weight, value_weight, pool_in_weight)
    pieces = in_one_piece((weights_in[0], weights_in[1], weights_in[2], weights_in[3]), SP, 0, 1)
    sums = tuple((jnp.dot(normed, piece, preferred_element_type=jnp.float32) for piece in pieces))
    query, key, value, pool_input = [total.astype(jnp.bfloat16) for total in sums]
    positions = offset + jnp.arange(tok_rows, dtype=jnp.int32)
    tables = rope_tables(positions, HD)
    rot_query = rotate_heads(query, tables, HD)
    rot_key = rotate_heads(key, tables, HD)
    chans = pool_input.shape[1]
    key_width = rot_key.shape[1]
    joined = jnp.concatenate([pool_input, rot_key, value], 1)
    extended = with_halo(joined, ((SP, 0),), WINDOW)
    pool_ext = extended[WINDOW - pool_reach : WINDOW + tok_rows + pool_reach, :chans]
    key_ext = extended[:, chans : chans + key_width]
    value_ext = extended[:, chans + key_width :]
    half_width = jnp.left_shift(jnp.int32(1), lax.axis_index("tp"))
    pooled = pool_group(pool_ext, pool_input, positions, half_width, seq_total)
    pool_out = jnp.dot(pooled, pool_mix_weight[0], preferred_element_type=jnp.float32).astype(
        jnp.bfloat16
    )
    heads_local = rot_query.shape[1] // HD
    kv_local = key_width // HD
    grp = heads_local // kv_local
    query_heads = rot_query.reshape(tok_rows, kv_local, grp, HD)
    key_heads = key_ext.reshape(-1, kv_local, HD)
    value_heads = value_ext.reshape(-1, kv_local, HD)
    sink = sink_logit.reshape(kv_local, grp)
    block_rows = min(tok_rows, 256)
    attended_parts = []
    log_parts = []
    for block_index in range(tok_rows // block_rows):
        start = block_index * block_rows
        query_pos = offset + start + jnp.arange(block_rows, dtype=jnp.int32)
        key_pos = offset + start - WINDOW + jnp.arange(block_rows + 2 * WINDOW, dtype=jnp.int32)
        attended_block, log_block = attend_block(
            query_heads[start : start + block_rows],
            key_heads[start : start + block_rows + 2 * WINDOW],
            value_heads[start : start + block_rows + 2 * WINDOW],
            sink,
            query_pos,
            key_pos,
            seq_total,
        )
        attended_parts.append(attended_block.reshape(block_rows, heads_local * HD))
        log_parts.append(log_block.reshape(heads_local, block_rows))
    attended = jnp.concatenate(attended_parts, 0)
    log_weight = jnp.concatenate(log_parts, 1)
    out_pool_full, out_attn_full = fetch_outputs(out_pool_weight, out_attn_weight)
    term = jnp.dot(pool_out, out_pool_full, preferred_element_type=jnp.float32)
    term = term + jnp.dot(attended, out_attn_full, preferred_element_type=jnp.float32)
    mixed = summed_on_arrival(term.astype(jnp.bfloat16), "tp", 1).astype(jnp.bfloat16)
    return (mixed, log_weight)


def solution(mesh):
    finer = Mesh(mesh.devices.reshape(8, 8, 2, mesh.shape["tp"]), ("sp_0", "sp_1", "sp_2", "tp"))
    placed = (
        P(SP, "tp"),
        P(),
        P(SP, "tp"),
        P(SP, "tp"),
        P(SP, "tp"),
        P(SP, "tp"),
        P("tp", None, None),
        P("tp"),
        P("tp", SP),
        P("tp", SP),
    )
    return jax.shard_map(
        local, mesh=finer, in_specs=placed, out_specs=(P(SP, "tp"), P("tp", SP)), check_vma=False
    )
```

profile of v0, /device:TPU:1, one launch (start us, length us, event | category | flops | bytes accessed | tf_op | source)
XLA Modules:
  0.0 189.5 jit_solution(7298341624987527233)
XLA Ops:
  7.2 1.4 pad_maximum_fusion.6
  8.7 1.3 copy.18
  9.9 1.5 broadcast_in_dim.176
  11.4 5.0 %all-to-all-start = ((bf16[4,512,512]{1,2,0:T(8,128)(2,1)}), bf16[4,512,512]{1,2,0:T(8,128)(2,1)S(1)}, u32[]{:S(2)}, u32[]{:S(2)}) async-start(bf16[4,512,512]{1,2,0:T(8,128)(2,1)} %broadcast_in_dim.176), calls=%async_computation | async-start | bytes 4194304 | tf_op jit(solution)/shard_map/all_to_all | solution.py:21
  16.4 20.5 %all-to-all-done = bf16[4,512,512]{1,2,0:T(8,128)(2,1)S(1)} async-done(((bf16[4,512,512]{1,2,0:T(8,128)(2,1)}), bf16[4,512,512]{1,2,0:T(8,128)(2,1)S(1)}, u32[]{:S(2)}, u32[]{:S(2)}) %all-to-all-start) | async-done | bytes 2097184 | tf_op jit(solution)/shard_map/all_to_all | solution.py:21
  37.0 1.4 broadcast_in_dim.193
  38.3 21.5 %all-to-all-start.1 = ((bf16[64,768,16]{1,2,0:T(8,128)(2,1)}), bf16[64,768,16]{1,2,0:T(8,128)(2,1)}, u32[]{:S(2)}, u32[]{:S(2)}) async-start(bf16[64,768,16]{1,2,0:T(8,128)(2,1)} %broadcast_in_dim.193), calls=%async_computation.1 | async-start | bytes 3145728 | tf_op jit(solution)/shard_map/all_to_all | solution.py:21
  59.9 0.1 max.38
  60.1 0.7 convert_add_fusion
  60.8 0.9 fusion.32
  61.7 0.9 fusion.34
  62.7 0.3 multiply_cosine_fusion.1
  63.0 0.5 multiply_reduce_fusion
  63.5 1.9 %fusion.1 = bf16[512,2048]{0,1:T(8,128)(2,1)} fusion(f32[2048]{0:T(1024)S(1)} %copy-done.12, f32[512]{0:T(512)S(1)} %add_rsqrt_fusion, bf16[4,512,512]{1,2,0:T(8,128)(2,1)S(1)} %all-to-all-done), kind=kLoop, calls=%fused_computation.2 | loop fusion | flops 4194304 | bytes 4204544 | tf_op jit(solution)/shard_map/convert_element_type | solution.py:179
  65.4 35.8 %all-to-all-done.1 = bf16[64,768,16]{1,2,0:T(8,128)(2,1)} async-done(((bf16[64,768,16]{1,2,0:T(8,128)(2,1)}), bf16[64,768,16]{1,2,0:T(8,128)(2,1)}, u32[]{:S(2)}, u32[]{:S(2)}) %all-to-all-start.1) | async-done | bytes 1572896 | tf_op jit(solution)/shard_map/all_to_all | solution.py:21
  101.1 1.6 broadcast_in_dim.194
  102.8 10.8 %all_to_all.20 = bf16[2,64,768,16]{2,3,1,0:T(8,128)(2,1)S(1)} all-to-all(bf16[2,64,768,16]{2,3,1,0:T(8,128)(2,1)S(1)} %broadcast_in_dim.194), channel_id=1, replica_groups=mesh['sp_0'=8,'sp_1'=8,'sp_2'=2,'tp'=4] {'sp_2'}, dimensions={0} | all-to-all | bytes 6291456 | tf_op jit(solution)/shard_map/all_to_all | solution.py:21
  113.6 0.5 copy.19
  114.1 1.0 slice.241
  115.1 0.3 slice.252
  115.4 3.6 %all-gather.2.cloned.1.call-done = bf16[2048,1024]{1,0:T(8,128)(2,1)} async-done(((bf16[16,1024]{1,0:T(8,128)(2,1)}), bf16[2048,1024]{1,0:T(8,128)(2,1)}) %all-gather.2.cloned.1.call-update) | async-done | bytes 4194320 | tf_op jit(solution)/shard_map/all_gather | solution.py:56
  119.0 3.7 %fusion.10 = bf16[512,512]{0,1:T(8,128)(2,1)S(1)} fusion(bf16[512,2048]{0,1:T(8,128)(2,1)} %fusion.1, bf16[2048,1024]{1,0:T(8,128)(2,1)} %all-gather.2.cloned.1.call-done), kind=kOutput, calls=%fused_computation.20 | convolution fusion | flops 1074003968 | bytes 4718592 | tf_op jit(solution)/shard_map/dot_general | solution.py:185
  122.7 0.1 convert.38
  122.8 0.3 copy-done.16
  123.1 0.5 convolution_convert_fusion.3
  123.6 0.2 subtract_convert_fusion.1
  123.9 0.8 convolution_convert_fusion.1
  124.6 0.5 convolution_convert_fusion.2
  125.2 3.5 %collective-permute-start = (bf16[128,512]{0,1:T(8,128)(2,1)S(1)}, bf16[128,512]{0,1:T(8,128)(2,1)S(1)}, u32[]{:S(2)}, u32[]{:S(2)}) collective-permute-start(bf16[128,512]{0,1:T(8,128)(2,1)S(1)} %get-tuple-element.33), channel_id=1, source_target_pairs={{0,4},{4,8},{8,12},{12,16},{16,20},{20,24},{24,28},{28,32},{32,36}... | collective-permute-start | bytes 393224 | tf_op jit(solution)/shard_map/ppermute | solution.py:68
  128.7 2.1 %collective-permute-start.1 = (bf16[128,512]{0,1:T(8,128)(2,1)S(1)}, bf16[128,512]{0,1:T(8,128)(2,1)S(1)}, u32[]{:S(2)}, u32[]{:S(2)}) collective-permute-start(bf16[128,512]{0,1:T(8,128)(2,1)S(1)} %get-tuple-element.34), channel_id=1, source_target_pairs={{4,0},{8,4},{12,8},{16,12},{20,16},{24,20},{28,24},{32,28},{36,32}... | collective-permute-start | bytes 393224 | tf_op jit(solution)/shard_map/ppermute | solution.py:70
  130.9 4.1 %collective-permute-done.1 = bf16[128,512]{0,1:T(8,128)(2,1)S(1)} collective-permute-done((bf16[128,512]{0,1:T(8,128)(2,1)S(1)}, bf16[128,512]{0,1:T(8,128)(2,1)S(1)}, u32[]{:S(2)}, u32[]{:S(2)}) %collective-permute-start.1) | collective-permute-done | bytes 131104 | tf_op jit(solution)/shard_map/ppermute | solution.py:70
  135.0 0.1 maximum_maximum_fusion
  135.2 0.8 fusion.4
  136.1 0.9 fusion.2
  137.0 0.8 fusion.5
  137.9 0.1 exponential_add_fusion.1
  138.0 0.9 fusion.3
  138.9 0.1 exponential_add_fusion
  138.9 1.9 %fusion.14 = bf16[2,64,4,256]{3,1,2,0:T(8,128)(2,1)} fusion(bf16[512,2,64,1]{0,2,3,1:T(8,128)(2,1)S(1)} %bitcast.110, f32[2,512,256,4]{2,1,3,0:T(8,128)S(1)} %get-tuple-element.52, f32[2,4,256]{2,1,0:T(4,128)S(1)} %get-tuple-element.45, f32[2,4,256]{2,1,0:T(4,128)S(1)} %broadcast_maximum_fusion.1, pred[256,512]{0,1:T(8,128)(4,1)S(1)} %copy-done.3), kind=kOutput, calls=%fused_computation.22 | convolution fusion | flops 139591680 | bytes 4734976 | tf_op jit(solution)/shard_map/hgqk,khd->qhgd/dot_general | solution.py:155
  140.9 1.9 %fusion.13 = bf16[2,64,4,256]{3,1,2,0:T(8,128)(2,1)} fusion(bf16[512,2,64,1]{0,2,3,1:T(8,128)(2,1)S(1)} %bitcast.109, f32[2,512,256,4]{2,1,3,0:T(8,128)S(1)} %get-tuple-element.54, f32[2,4,256]{2,1,0:T(4,128)S(1)} %exponential_add_fusion, f32[2,4,256]{2,1,0:T(4,128)S(1)} %get-tuple-element.46, pred[256,512]{0,1:T(8,128)(4,1)S(1)} %copy-done.2), kind=kOutput, calls=%fused_computation.21 | convolution fusion | flops 139591680 | bytes 4734976 | tf_op jit(solution)/shard_map/hgqk,khd->qhgd/dot_general | solution.py:155
  142.8 5.7 %fusion.15 = f32[512,2048]{1,0:T(8,128)} fusion(bf16[256,2048]{0,1:T(8,128)(2,1)} %bitcast.100, bf16[512,256]{0,1:T(8,128)(2,1)} %copy-done.4, bf16[640,512]{0,1:T(8,128)(2,1)S(1)} %get-tuple-element.32, bf16[640,512]{0,1:T(8,128)(2,1)S(1)} %get-tuple-element.31, f32[512]{0:T(512)} %get-tuple-element.2, pred[512]{0:T(512)(128)(4,1)} %get-tuple-element.18, ...), kind=kOutput, calls=%fused_computation.25 | convolution fusion | flops 610664448 | bytes 9578496 | tf_op jit(solution)/shard_map/dot_general | solution.py:231
  148.6 3.7 %add_convert_fusion = bf16[512,2048]{1,0:T(8,128)(2,1)S(1)} fusion(f32[512,2048]{1,0:T(8,128)} %fusion.15, bf16[512,2048]{0,1:T(8,128)(2,1)S(1)} %bitcast.95, bf16[256,512]{0,1:T(8,128)(2,1)} %bitcast.107, bf16[256,512]{0,1:T(8,128)(2,1)} %bitcast.106), kind=kOutput, calls=%fused_computation.5 | convolution fusion | flops 1076887552 | bytes 8912896 | tf_op jit(solution)/shard_map/dot_general | solution.py:232
  152.3 1.5 copy.31
  153.8 3.6 %all-to-all-start.3 = ((bf16[4,512,512]{2,1,0:T(8,128)(2,1)}), bf16[4,512,512]{2,1,0:T(8,128)(2,1)S(1)}, u32[]{:S(2)}, u32[]{:S(2)}) async-start(bf16[4,512,512]{2,1,0:T(8,128)(2,1)} %bitcast.97), calls=%async_computation.3 | async-start | bytes 4194304 | tf_op jit(solution)/shard_map/all_to_all | solution.py:85
  157.5 0.1 log_add_fusion.1
  157.6 0.6 pad_maximum_fusion.8
  158.2 23.2 %all-to-all-done.3 = bf16[4,512,512]{2,1,0:T(8,128)(2,1)S(1)} async-done(((bf16[4,512,512]{2,1,0:T(8,128)(2,1)}), bf16[4,512,512]{2,1,0:T(8,128)(2,1)S(1)}, u32[]{:S(2)}, u32[]{:S(2)}) %all-to-all-start.3) | async-done | bytes 2097184 | tf_op jit(solution)/shard_map/all_to_all | solution.py:85
  181.4 1.2 reduce_sum.46
  (59 shorter events, 0.5 us)
Async XLA Ops:
  7.2 135.7 %copy-start = (bf16[1,256,256]{2,1,0:T(8,128)(2,1)S(1)}, bf16[1,256,256]{2,1,0:T(8,128)(2,1)}, u32[]{:S(2)}) copy-start(bf16[1,256,256]{2,1,0:T(8,128)(2,1)} %param.16) | copy-start | bytes 393220
  7.2 9.2 %copy-start.13 = (bf16[256,16]{0,1:T(8,128)(2,1)S(1)}, bf16[256,16]{0,1:T(8,128)(2,1)}, u32[]{:S(2)}) copy-start(bf16[256,16]{0,1:T(8,128)(2,1)} %param.18) | copy-start | bytes 24580
  7.2 9.2 %copy-start.9 = (bf16[512,16]{0,1:T(8,128)(2,1)S(1)}, bf16[512,16]{0,1:T(8,128)(2,1)}, u32[]{:S(2)}) copy-start(bf16[512,16]{0,1:T(8,128)(2,1)} %param.19) | copy-start | bytes 49156
  7.2 111.8 %all-gather.2.cloned.1.call-start = ((), (), s32[]{:S(2)}) async-start(), calls=%async_computation.4 | async-start | bytes 4227072 | tf_op jit(solution)/shard_map/all_gather | solution.py:56
  11.4 48.4 %copy-start.14 = (f32[8]{0:T(128)S(1)}, f32[8]{0:T(128)}, u32[]{:S(2)}) copy-start(f32[8]{0:T(128)} %param.17) | copy-start | bytes 100
  11.4 25.5 %all-to-all-start = ((bf16[4,512,512]{1,2,0:T(8,128)(2,1)}), bf16[4,512,512]{1,2,0:T(8,128)(2,1)S(1)}, u32[]{:S(2)}, u32[]{:S(2)}) async-start(bf16[4,512,512]{1,2,0:T(8,128)(2,1)} %broadcast_in_dim.176), calls=%async_computation | async-start | bytes 4194304 | tf_op jit(solution)/shard_map/all_to_all | solution.py:21
  16.4 47.1 %copy-start.12 = (f32[2048]{0:T(1024)S(1)}, f32[2048]{0:T(1024)}, u32[]{:S(2)}) copy-start(f32[2048]{0:T(1024)} %param.11) | copy-start | bytes 24580
  38.3 62.8 %all-to-all-start.1 = ((bf16[64,768,16]{1,2,0:T(8,128)(2,1)}), bf16[64,768,16]{1,2,0:T(8,128)(2,1)}, u32[]{:S(2)}, u32[]{:S(2)}) async-start(bf16[64,768,16]{1,2,0:T(8,128)(2,1)} %broadcast_in_dim.193), calls=%async_computation.1 | async-start | bytes 3145728 | tf_op jit(solution)/shard_map/all_to_all | solution.py:21
  60.0 76.1 %copy-start.10 = (f32[2,4]{1,0:T(2,128)}, f32[2,4]{1,0:T(2,128)S(1)}, u32[]{:S(2)}) copy-start(f32[2,4]{1,0:T(2,128)S(1)} %max.38) | copy-start | bytes 100
  119.0 3.8 %copy-start.1 = (bf16[512,2048]{0,1:T(8,128)(2,1)S(1)}, bf16[512,2048]{0,1:T(8,128)(2,1)}, u32[]{:S(2)}) copy-start(bf16[512,2048]{0,1:T(8,128)(2,1)} %fusion.1) | copy-start | bytes 6291460
  119.0 4.1 %copy-start.16 = (bf16[2048,1024]{1,0:T(8,128)(2,1)S(1)}, bf16[2048,1024]{1,0:T(8,128)(2,1)}, u32[]{:S(2)}) copy-start(bf16[2048,1024]{1,0:T(8,128)(2,1)} %all-gather.2.cloned.1.call-done) | copy-start | bytes 12582916
  124.6 10.5 %copy-start.4 = (bf16[512,256]{0,1:T(8,128)(2,1)}, bf16[512,256]{0,1:T(8,128)(2,1)S(1)}, u32[]{:S(2)}) copy-start(bf16[512,256]{0,1:T(8,128)(2,1)S(1)} %convolution_convert_fusion.1) | copy-start | bytes 786436
  124.6 10.6 %copy-start.3 = (pred[256,512]{0,1:T(8,128)(4,1)S(1)}, pred[256,512]{0,1:T(8,128)(4,1)}, u32[]{:S(2)}) copy-start(pred[256,512]{0,1:T(8,128)(4,1)} %fusion.32) | copy-start | bytes 393220
  125.2 5.7 %collective-permute-start = (bf16[128,512]{0,1:T(8,128)(2,1)S(1)}, bf16[128,512]{0,1:T(8,128)(2,1)S(1)}, u32[]{:S(2)}, u32[]{:S(2)}) collective-permute-start(bf16[128,512]{0,1:T(8,128)(2,1)S(1)} %get-tuple-element.33), channel_id=1, source_target_pairs={{0,4},{4,8},{8,12},{12,16},{16,20},{20,24},{24,28},{28,32},{32,36}... | collective-permute-start | bytes 393224 | tf_op jit(solution)/shard_map/ppermute | solution.py:68
  128.7 6.3 %collective-permute-start.1 = (bf16[128,512]{0,1:T(8,128)(2,1)S(1)}, bf16[128,512]{0,1:T(8,128)(2,1)S(1)}, u32[]{:S(2)}, u32[]{:S(2)}) collective-permute-start(bf16[128,512]{0,1:T(8,128)(2,1)S(1)} %get-tuple-element.34), channel_id=1, source_target_pairs={{4,0},{8,4},{12,8},{16,12},{20,16},{24,20},{28,24},{32,28},{36,32}... | collective-permute-start | bytes 393224 | tf_op jit(solution)/shard_map/ppermute | solution.py:70
  135.2 1.8 copy-start.2
  136.1 1.7 copy-start.11
  137.0 1.8 copy-start.7
  138.8 2.0 %copy-start.5 = (f32[2,4,256]{2,1,0:T(4,128)}, f32[2,4,256]{2,1,0:T(4,128)S(1)}, u32[]{:S(2)}) copy-start(f32[2,4,256]{2,1,0:T(4,128)S(1)} %fusion.3) | copy-start | bytes 24580
  152.3 5.2 %copy-start.6 = (f32[2,4,256]{2,1,0:T(4,128)S(1)}, f32[2,4,256]{2,1,0:T(4,128)}, u32[]{:S(2)}) copy-start(f32[2,4,256]{2,1,0:T(4,128)} %copy-done.5) | copy-start | bytes 24580
  152.3 5.2 %copy-start.8 = (f32[2,4,256]{2,1,0:T(4,128)S(1)}, f32[2,4,256]{2,1,0:T(4,128)}, u32[]{:S(2)}) copy-start(f32[2,4,256]{2,1,0:T(4,128)} %copy-done.7) | copy-start | bytes 24580
  152.3 5.2 %copy-start.15 = (f32[8]{0:T(128)S(1)}, f32[8]{0:T(128)}, u32[]{:S(2)}) copy-start(f32[8]{0:T(128)} %param.17) | copy-start | bytes 100
  153.8 27.6 %all-to-all-start.3 = ((bf16[4,512,512]{2,1,0:T(8,128)(2,1)}), bf16[4,512,512]{2,1,0:T(8,128)(2,1)S(1)}, u32[]{:S(2)}, u32[]{:S(2)}) async-start(bf16[4,512,512]{2,1,0:T(8,128)(2,1)} %bitcast.97), calls=%async_computation.3 | async-start | bytes 4194304 | tf_op jit(solution)/shard_map/all_to_all | solution.py:85
Sparse Core Ops, SparseCore 0:
  11.7 107.2 all-gather.1
where the time goes:
time: 191 us; the launch traced here: 189 us
  waiting for transfers between devices  87.2 us (46%)
  starting transfers between devices  35.7 us (19%)
  matrix products  20.3 us (11%)
  between operations  14.6 us (8%)
  other arithmetic  11.2 us (6%)
  blocking collectives  10.8 us (6%)
  local copies, waits for them, and re-layouts  9.59 us (5%)
    all_to_all x2, waiting for transfers between devices, sent_to_all(): lax.all_to_all(jnp.broadcast_to(shard[None], (count, *shard.shape)), axis...  56.3 us
    all_to_all x2, starting transfers between devices, sent_to_all(): lax.all_to_all(jnp.broadcast_to(shard[None], (count, *shard.shape)), axis...  26.4 us
    all_to_all x1, waiting for transfers between devices, summed_on_arrival(): lax.all_to_all(in_blocks(shard, dim, count), axis, 0, 0, tiled=True)  23.2 us
    all_to_all x1, blocking collectives, sent_to_all(): lax.all_to_all(jnp.broadcast_to(shard[None], (count, *shard.shape)), axis...  10.8 us
    dot_general x1, matrix products, local(): term = jnp.dot(pool_out, out_pool_full, preferred_element_type=jnp.float32)  5.74 us
    dot_general x4, matrix products, local(): jnp.dot(normed, piece, preferred_element_type=jnp.float32)  5.4 us
    broadcast_in_dim x3, local copies, waits for them, and re-layouts, sent_to_all(): jnp.broadcast_to(shard[None], (count, *shard.shape))  4.5 us
    ppermute x1, waiting for transfers between devices, with_halo(): lax.ppermute(head, axis, [((i + 1) % count, i) for i in range(ends)])  4.08 us
  transfers between devices with their start and end apart: 6, of which 5 were waited for; matrix products, arithmetic and copies ran while one was open for 7% of the time, Pallas kernels for 0%

commit v1 on v0

--- a/solution.py
+++ b/solution.py
@@ -2,6 +2,8 @@
 import jax.numpy as jnp
 from jax import lax
 from jax.sharding import Mesh
+from jax.experimental import pallas as pl
+from jax.experimental.pallas import tpu as pltpu
 from jax.sharding import PartitionSpec as P
 
 HD = 64
@@ -14,47 +16,6 @@
 rope_base = 10000.0
 pool_reach = 8
 neg_fill = -1e30
-
-
-def sent_to_all(shard, axis):
-    count = lax.axis_size(axis)
-    return lax.all_to_all(
-        jnp.broadcast_to(shard[None], (count, *shard.shape)), axis, 0, 0, tiled=True
-    )
-
-
-def laid_out(blocks, dim):
-    lengths = list(blocks.shape[1:])
-    lengths[dim] *= blocks.shape[0]
-    return jnp.moveaxis(blocks, 0, dim).reshape(lengths)
-
-
-def gathered_by_axis(shard, axes, dim):
-    far, near = axes
-    first = sent_to_all(shard, far)
-    blocks = jnp.swapaxes(sent_to_all(first, near), 0, 1)
-    return laid_out(blocks.reshape(-1, *shard.shape), dim)
-
-
-def side_by_side(arrays, axis, dim, along):
-    both = jnp.concatenate(arrays, axis=along)
-    out, at, gathered = (gathered_by_axis(both, axis, dim), 0, [])
-    for a in arrays:
-        gathered.append(lax.slice_in_dim(out, at, at + a.shape[along], axis=along))
-        at += a.shape[along]
-    return tuple(gathered)
-
-
-def collect(shard, axis, dim):
-    blocks = sent_to_all(shard, axis)
-    return laid_out(blocks, dim)
-
-
-def in_one_piece(arrays, axis, dim, along):
-    widths = [a.shape[along] for a in arrays]
-    both = jnp.concatenate(arrays, axis=along)
-    out = lax.all_gather(both, axis, axis=dim, tiled=True)
-    return tuple(jnp.split(out, [sum(widths[:k]) for k in range(1, len(widths))], axis=along))
 
 
 def with_halo(cells, sides, width):
@@ -86,6 +47,241 @@
     return jnp.sum(blocks.astype(jnp.float32), axis=0)
 
 
+MESH = pl.DeviceIdType.MESH
+AX_Z, AX_Y, AX_C, AX_X = "sp_0", "sp_1", "sp_2", "tp"
+
+
+def remote(src, dst, send_sem, recv_sem, device):
+    return pltpu.make_async_remote_copy(
+        src_ref=src,
+        dst_ref=dst,
+        send_sem=send_sem,
+        recv_sem=recv_sem,
+        device_id=device,
+        device_id_type=MESH,
+    )
+
+
+def wait_bytes(ref, sem):
+    pltpu.make_async_copy(ref, ref, sem).wait()
+
+
+class Torus:
+    def __init__(self, buf, first, sems):
+        self.buf, self.first = buf, first
+        self.p1_send, self.p1_recv, self.p2_send, self.p2_recv, self.d_send, self.d_recv = sems
+        self.z, self.y, self.c = lax.axis_index(AX_Z), lax.axis_index(AX_Y), lax.axis_index(AX_C)
+        self.n1 = buf.shape[1] if first == AX_Y else buf.shape[0]
+        self.n2 = buf.shape[0] if first == AX_Y else buf.shape[1]
+        self.a = self.y if first == AX_Y else self.z
+        self.b = self.z if first == AX_Y else self.y
+        self.second = AX_Z if first == AX_Y else AX_Y
+
+    def own(self):
+        return self.buf.at[self.z, self.y, self.c]
+
+    def chunk(self, b, start, size):
+        if self.first == AX_Y:
+            return self.buf.at[b, start : start + size, self.c]
+        return self.buf.at[start : start + size, b, self.c]
+
+    def hops(self, way, group):
+        half = self.n2 // 2
+        return half if (way == 0) == (group == 0) else half - 1
+
+    def phase1_start(self):
+        for d in range(1, self.n1):
+            remote(
+                self.own(), self.own(), self.p1_send, self.p1_recv,
+                {self.first: lax.rem(self.a + d, self.n1)},
+            ).start()
+
+    def phase1_wait(self):
+        wait_bytes(self.chunk(self.b, 0, self.n1 - 1), self.p1_recv)
+        self.to_partner(self.chunk(self.b, 0, self.n1))
+
+    def to_partner(self, ref):
+        remote(ref, ref, self.d_send, self.d_recv, {AX_C: 1 - self.c}).start()
+
+    def relay(self, way, group, hop):
+        step = 1 if way == 0 else self.n2 - 1
+        origin = lax.rem(self.b + (hop - 1) * (self.n2 - step), self.n2)
+        size = self.n1 // 2
+        ref = self.chunk(origin, group * size, size)
+        return remote(
+            ref, ref, self.p2_send.at[way, group, hop - 1], self.p2_recv.at[way, group, hop - 1],
+            {self.second: lax.rem(self.b + step, self.n2)},
+        )
+
+    def arrived(self, way, group, hop):
+        step = 1 if way == 0 else self.n2 - 1
+        origin = lax.rem(self.b + hop * (self.n2 - step), self.n2)
+        size = self.n1 // 2
+        ref = self.chunk(origin, group * size, size)
+        wait_bytes(ref, self.p2_recv.at[way, group, hop - 1])
+        self.to_partner(ref)
+
+    def level(self, hop):
+        for group in range(2):
+            for way in range(2):
+                last = self.hops(way, group)
+                if 1 < hop <= last + 1:
+                    self.arrived(way, group, hop - 1)
+                if hop <= last:
+                    self.relay(way, group, hop).start()
+
+    def levels(self):
+        return self.n2 // 2 + 1
+
+    def finish(self):
+        wait_bytes(self.buf.at[:, :, 1 - self.c], self.d_recv)
+        wait_bytes(self.buf.at[:, :, self.c], self.d_send)
+        wait_bytes(self.chunk(self.b, 0, self.n1 - 1), self.p1_send)
+        for group in range(2):
+            for way in range(2):
+                for hop in range(1, self.hops(way, group) + 1):
+                    self.relay(way, group, hop).wait_send()
+
+
+def torus_sems(n2):
+    dma = pltpu.SemaphoreType.DMA
+    hops = max(n2 // 2, 1)
+    return [dma(()), dma(()), dma((2, 2, hops)), dma((2, 2, hops)), dma(()), dma(())]
+
+
+class Ring:
+    def __init__(self, buf, sems):
+        self.buf = buf
+        self.send, self.recv = sems
+        self.n, self.x = buf.shape[0], lax.axis_index(AX_X)
+        self.half = buf.shape[1] // 2
+
+    def part(self, x, which):
+        return self.buf.at[x, which * self.half : (which + 1) * self.half]
+
+    def copy(self, way, index, x, which):
+        step = 1 if way == 0 else self.n - 1
+        ref = self.part(x, which)
+        return remote(
+            ref, ref, self.send.at[way, index], self.recv.at[way, index],
+            {AX_X: lax.rem(self.x + step, self.n)},
+        )
+
+    def start(self):
+        for index in range(2):
+            for way in range(2):
+                self.copy(way, index, self.x, index if way == 0 else 1 - index).start()
+
+    def forward(self):
+        for way in range(2):
+            step = 1 if way == 0 else self.n - 1
+            behind = lax.rem(self.x + self.n - step, self.n)
+            which = way
+            wait_bytes(self.part(behind, which), self.recv.at[way, 0])
+            self.copy(way, 2, behind, which).start()
+
+    def finish(self):
+        for way in range(2):
+            step = 1 if way == 0 else self.n - 1
+            behind = lax.rem(self.x + self.n - step, self.n)
+            across = lax.rem(self.x + 2, self.n)
+            wait_bytes(self.part(behind, 1 - way), self.recv.at[way, 1])
+            wait_bytes(self.part(across, way), self.recv.at[way, 2])
+        for way in range(2):
+            for index in range(3):
+                self.copy(way, index, self.x, 0).wait_send()
+
+
+def greet(peers):
+    barrier = pltpu.get_barrier_semaphore()
+    for peer in peers:
+        pl.semaphore_signal(barrier, inc=1, device_id=peer, device_id_type=MESH)
+    pl.semaphore_wait(barrier, len(peers))
+
+
+def all_peers(nz, ny, nx):
+    z, y, c, x = (lax.axis_index(a) for a in (AX_Z, AX_Y, AX_C, AX_X))
+    peers = [{AX_C: 1 - c}]
+    peers += [{AX_X: lax.rem(x + d, nx)} for d in (1, nx - 1)]
+    peers += [{AX_Y: lax.rem(y + d, ny)} for d in range(1, ny)]
+    peers += [{AX_Z: lax.rem(z + d, nz)} for d in range(1, nz)]
+    return peers
+
+
+def gather_kernel(
+    tok_ref, q_ref, k_ref, v_ref, p_ref, oa_ref, ob_ref,
+    t_buf, wa, wb, oa, ob, load_sem, ring_send, ring_recv, *torus,
+):
+    z, y, c, x = (lax.axis_index(a) for a in (AX_Z, AX_Y, AX_C, AX_X))
+    ring = Ring(t_buf, (ring_send, ring_recv))
+    in_a = Torus(wa, AX_Y, torus[0:6])
+    in_b = Torus(wb, AX_Z, torus[6:12])
+    out_a = Torus(oa, AX_Y, torus[12:18])
+    out_b = Torus(ob, AX_Z, torus[18:24])
+    loads = [
+        pltpu.make_async_copy(tok_ref, t_buf.at[x], load_sem.at[0]),
+        pltpu.make_async_copy(q_ref, wa.at[z, y, c], load_sem.at[1]),
+        pltpu.make_async_copy(k_ref, wb.at[z, y, c, :, 0:128], load_sem.at[2]),
+        pltpu.make_async_copy(v_ref, wb.at[z, y, c, :, 128:256], load_sem.at[3]),
+        pltpu.make_async_copy(p_ref, wb.at[z, y, c, :, 256:512], load_sem.at[4]),
+        pltpu.make_async_copy(oa_ref, oa.at[z, y, c], load_sem.at[5]),
+        pltpu.make_async_copy(ob_ref, ob.at[z, y, c], load_sem.at[6]),
+    ]
+    for load in loads:
+        load.start()
+    greet(all_peers(wa.shape[0], wa.shape[1], t_buf.shape[0]))
+    for load in loads:
+        load.wait()
+    ring.start()
+    in_a.phase1_start()
+    in_b.phase1_start()
+    in_a.phase1_wait()
+    in_b.phase1_wait()
+    for hop in range(1, in_a.levels() + 1):
+        in_a.level(hop)
+        in_b.level(hop)
+        if hop == 2:
+            ring.forward()
+        if hop == in_a.levels() - 1:
+            out_a.phase1_start()
+            out_b.phase1_start()
+    out_a.phase1_wait()
+    out_b.phase1_wait()
+    for hop in range(1, out_a.levels() + 1):
+        out_a.level(hop)
+        out_b.level(hop)
+    ring.finish()
+    in_a.finish()
+    in_b.finish()
+    out_a.finish()
+    out_b.finish()
+
+
+def gather_all(tokens, weights, out_a, out_b):
+    nz, ny, nc, nx = (lax.axis_size(a) for a in (AX_Z, AX_Y, AX_C, AX_X))
+    rows, width = tokens.shape
+    bf = jnp.bfloat16
+    shapes = [
+        jax.ShapeDtypeStruct((nx, rows, width), bf),
+        jax.ShapeDtypeStruct((nz, ny, nc, 16, 512), bf),
+        jax.ShapeDtypeStruct((nz, ny, nc, 16, 512), bf),
+        jax.ShapeDtypeStruct((nz, ny, nc, 16, 384), bf),
+        jax.ShapeDtypeStruct((nz, ny, nc, 16, 384), bf),
+    ]
+    dma = pltpu.SemaphoreType.DMA
+    return pl.pallas_call(
+        gather_kernel,
+        out_shape=shapes,
+        in_specs=[pl.BlockSpec(memory_space=pl.ANY)] * 7,
+        out_specs=[pl.BlockSpec(memory_space=pltpu.VMEM)] * 5,
+        scratch_shapes=[dma((7,)), dma((2, 3)), dma((2, 3))]
+        + torus_sems(nz) + torus_sems(ny) + torus_sems(nz) + torus_sems(ny),
+        compiler_params=pltpu.CompilerParams(
+            collective_id=0, has_side_effects=True, vmem_limit_bytes=40 * 1024 * 1024
+        ),
+    )(tokens, *weights, out_a, out_b)
+
+
 def rope_tables(positions, head_dim):
     n_freq = head_dim // 4
     freqs = rope_base ** (-jnp.arange(n_freq, dtype=jnp.float32) / n_freq)
@@ -154,10 +350,6 @@
     weights = (exps / row_total[..., None]).astype(jnp.bfloat16)
     attended = jnp.einsum("hgqk,khd->qhgd", weights, values, preferred_element_type=jnp.float32)
     return (attended.astype(jnp.bfloat16), row_top + jnp.log(row_total))
-
-
-def fetch_outputs(out_pool_weight, out_attn_weight):
-    return side_by_side((out_pool_weight, out_attn_weight), (("sp_0", "sp_1"), "sp_2"), 1, 0)
 
 
 def local(
@@ -172,7 +364,14 @@
     out_pool_weight,
     out_attn_weight,
 ):
-    whole = collect(tokens, "tp", 1)
+    out_rows = jnp.concatenate([out_pool_weight, out_attn_weight], 0).T
+    blocks, wa, wb, oa, ob = gather_all(
+        tokens,
+        (query_weight, key_weight, value_weight, pool_in_weight),
+        out_rows[:, :384],
+        out_rows[:, 384:],
+    )
+    whole = jnp.moveaxis(blocks, 0, 1).reshape(blocks.shape[1], -1)
     wide = whole.astype(jnp.float32)
     normed = (
         wide * lax.rsqrt(jnp.mean(wide * wide, -1, keepdims=True) + norm_eps) * norm_gain
@@ -180,8 +379,8 @@
     tok_rows = normed.shape[0]
     seq_total = tok_rows * lax.axis_size(SP)
     offset = lax.axis_index(SP) * tok_rows
-    weights_in = (query_weight, key_weight, value_weight, pool_in_weight)
-    pieces = in_one_piece((weights_in[0], weights_in[1], weights_in[2], weights_in[3]), SP, 0, 1)
+    weight_a, weight_b = wa.reshape(-1, 512), wb.reshape(-1, 512)
+    pieces = (weight_a, weight_b[:, :128], weight_b[:, 128:256], weight_b[:, 256:])
     sums = tuple((jnp.dot(normed, piece, preferred_element_type=jnp.float32) for piece in pieces))
     query, key, value, pool_input = [total.astype(jnp.bfloat16) for total in sums]
     positions = offset + jnp.arange(tok_rows, dtype=jnp.int32)
@@ -227,9 +426,13 @@
         log_parts.append(log_block.reshape(heads_local, block_rows))
     attended = jnp.concatenate(attended_parts, 0)
     log_weight = jnp.concatenate(log_parts, 1)
-    out_pool_full, out_attn_full = fetch_outputs(out_pool_weight, out_attn_weight)
-    term = jnp.dot(pool_out, out_pool_full, preferred_element_type=jnp.float32)
-    term = term + jnp.dot(attended, out_attn_full, preferred_element_type=jnp.float32)
+    features = jnp.concatenate([pool_out, attended], 1)
+    outs = (((1,), (1,)), ((), ()))
+    term = lax.dot_general(
+        features[:, :384], oa.reshape(-1, 384), outs, preferred_element_type=jnp.float32
+    ) + lax.dot_general(
+        features[:, 384:], ob.reshape(-1, 384), outs, preferred_element_type=jnp.float32
+    )
     mixed = summed_on_arrival(term.astype(jnp.bfloat16), "tp", 1).astype(jnp.bfloat16)
     return (mixed, log_weight)
 

time: 191 us -> 140 us (0.73)
  waiting for transfers between devices: 87.2 us -> 26 us
  Pallas kernels: 0 us -> 60.2 us
  starting transfers between devices: 35.7 us -> 8.53 us
  between operations: 14.6 us -> 1.11 us
  blocking collectives: 10.8 us -> 0 us
  matrix products: 20.3 us -> 13.2 us
  local copies, waits for them, and re-layouts: 9.59 us -> 16 us
  other arithmetic: 11.2 us -> 14.3 us
    pallas_call x0 -> x1, Pallas kernels: none -> 60.2 us  [gather_all(): pl.pallas_call(gather_kernel, out_shape=shapes, in_specs=[pl.BlockSpec(me...]
    all_to_all x2 -> x0, waiting for transfers between devices: 56.3 us -> none  [sent_to_all(): lax.all_to_all(jnp.broadcast_to(shard[None], (count, *shard.shape)), axis...]
    all_to_all x2 -> x0, starting transfers between devices: 26.4 us -> none  [sent_to_all(): lax.all_to_all(jnp.broadcast_to(shard[None], (count, *shard.shape)), axis...]
    all_to_all x1 -> x0, blocking collectives: 10.8 us -> none  [sent_to_all(): lax.all_to_all(jnp.broadcast_to(shard[None], (count, *shard.shape)), axis...]
    convert_element_type x0 -> x1, local copies, waits for them, and re-layouts: none -> 5.31 us  [local(): wide = whole.astype(jnp.float32)]
    dot_general x2 -> x3, matrix products: 9.41 us -> 4.48 us  [the longest x1 1.87 us: local(): jnp.dot(pooled, pool_mix_weight[0], preferred_element_type=jnp.float32)]
    broadcast_in_dim x3 -> x0, local copies, waits for them, and re-layouts: 4.5 us -> none  [sent_to_all(): jnp.broadcast_to(shard[None], (count, *shard.shape))]
    mul x0 -> x2, local copies, waits for them, and re-layouts: none -> 4.32 us  [local(): wide * lax.rsqrt(jnp.mean(wide * wide, -1, keepdims=True) + norm_eps)]
  transfers between devices with their start and end apart: 6 -> 3, of which waited for: 5 -> 1; matrix products, arithmetic and copies ran while one was open for 7% -> 8% of each run, Pallas kernels for 0% -> 0%
where the time goes in v1:
time: 140 us; the launch traced here: 139 us
  Pallas kernels  60.2 us (43%)
  waiting for transfers between devices  26 us (19%)
  local copies, waits for them, and re-layouts  16 us (11%)
  other arithmetic  14.3 us (10%)
  matrix products  13.2 us (9%)
  starting transfers between devices  8.53 us (6%)
    pallas_call x1, Pallas kernels, gather_all(): pl.pallas_call(gather_kernel, out_shape=shapes, in_specs=[pl.BlockSpec(me...  60.2 us
    all_to_all x1, waiting for transfers between devices, summed_on_arrival(): lax.all_to_all(in_blocks(shard, dim, count), axis, 0, 0, tiled=True)  26 us
    convert_element_type x1, local copies, waits for them, and re-layouts, local(): wide = whole.astype(jnp.float32)  5.31 us
    unnamed x32, local copies, waits for them, and re-layouts  4.65 us
    dot_general x4, matrix products, local(): jnp.dot(normed, piece, preferred_element_type=jnp.float32)  4.62 us
    mul x2, local copies, waits for them, and re-layouts, local(): wide * lax.rsqrt(jnp.mean(wide * wide, -1, keepdims=True) + norm_eps)  4.32 us
    all_to_all x1, starting transfers between devices, summed_on_arrival(): lax.all_to_all(in_blocks(shard, dim, count), axis, 0, 0, tiled=True)  4.09 us
    convert_element_type x1, other arithmetic, local(): wide = whole.astype(jnp.float32)  3.02 us
  transfers between devices with their start and end apart: 3, of which 1 were waited for; matrix products, arithmetic and copies ran while one was open for 8% of the time, Pallas kernels for 0%

profile of v1, /device:TPU:1, one launch (start us, length us, event | category | flops | bytes accessed | tf_op | source)
XLA Modules:
  0.0 139.4 jit_solution(15113453512872531827)
XLA Ops:
  0.7 0.8 maximum_bitcast_fusion
  1.4 1.0 copy-done.5
  2.5 0.7 copy-done.6
  3.2 0.7 copy-done.7
  3.9 0.7 copy-done.8
  4.6 0.7 copy-done.9
  5.3 60.2 %shard_map.113 = (bf16[4,512,512]{2,1,0:T(8,128)(2,1)S(1)}, bf16[8,8,2,16,512]{4,3,2,1,0:T(8,128)(2,1)S(1)}, bf16[8,8,2,16,512]{4,3,2,1,0:T(8,128)(2,1)S(1)}, bf...) custom-call(bf16[512,512]{1,0:T(8,128)(2,1)S(1)} %copy-done.5, bf16[16,512]{1,0:T(8,128)(2,1)S(1)} %copy-done.6, ...), custom_call_target="tpu_custom_call" | custom-call | tf_op jit(solution)/shard_map/pallas_call | solution.py:272
  65.5 0.5 fusion
  66.0 3.0 %convert_bitcast_fusion = f32[512,4,512]{2,0,1:T(8,128)} fusion(bf16[4,512,512]{2,1,0:T(8,128)(2,1)S(1)} %get-tuple-element.7), kind=kLoop, calls=%fused_computation.2 | loop fusion | flops 1048576 | bytes 6291456 | tf_op jit(solution)/shard_map/convert_element_type | solution.py:375
  69.1 0.6 copy-done.12
  69.6 5.3 %copy.18 = f32[512,4,512]{0,2,1:T(8,128)} copy(f32[512,4,512]{2,0,1:T(8,128)} %convert_bitcast_fusion) | data formatting | bytes 8388608 | tf_op jit(solution)/shard_map/convert_element_type | solution.py:375
  74.9 2.8 %fusion.4 = bf16[512,2048]{0,1:T(8,128)(2,1)S(1)} fusion(f32[512,4,512]{0,2,1:T(8,128)} %copy.18, f32[2048]{0:T(1024)S(1)} %copy-done.14, f32[512]{0:T(512)S(1)} %add_rsqrt_fusion), kind=kLoop, calls=%fused_computation.10 | loop fusion | flops 3145728 | bytes 6301696 | tf_op jit(solution)/shard_map/convert_element_type | solution.py:378
  77.7 0.1 copy-done.13
  77.8 0.5 convolution_convert_fusion.4
  78.3 0.8 convolution_convert_fusion.2
  79.0 0.5 convolution_convert_fusion.3
  79.6 0.3 multiply_cosine_fusion.1
  80.0 2.5 %collective-permute-start = (bf16[128,512]{0,1:T(8,128)(2,1)S(1)}, bf16[128,512]{0,1:T(8,128)(2,1)S(1)}, u32[]{:S(2)}, u32[]{:S(2)}) collective-permute-start(bf16[128,512]{0,1:T(8,128)(2,1)S(1)} %get-tuple-element.43), channel_id=1, source_target_pairs={{0,4},{4,8},{8,12},{12,16},{16,20},{20,24},{24,28},{28,32},{32,36}... | collective-permute-start | bytes 393224 | tf_op jit(solution)/shard_map/ppermute | solution.py:29
  82.5 1.9 %collective-permute-start.1 = (bf16[128,512]{0,1:T(8,128)(2,1)S(1)}, bf16[128,512]{0,1:T(8,128)(2,1)S(1)}, u32[]{:S(2)}, u32[]{:S(2)}) collective-permute-start(bf16[128,512]{0,1:T(8,128)(2,1)S(1)} %get-tuple-element.44), channel_id=1, source_target_pairs={{4,0},{8,4},{12,8},{16,12},{20,16},{24,20},{28,24},{32,28},{36,32}... | collective-permute-start | bytes 393224 | tf_op jit(solution)/shard_map/ppermute | solution.py:31
  84.5 1.9 %fusion.9 = bf16[512,4,512]{2,0,1:T(8,128)(2,1)} fusion(bf16[4,512,512]{2,1,0:T(8,128)(2,1)S(1)} %get-tuple-element.7, f32[4,512]{1,0:T(4,128)S(1)} %mul.237, f32[512]{0:T(512)S(1)} %add_rsqrt_fusion), kind=kLoop, calls=%fused_computation.20 | loop fusion | flops 4194304 | bytes 4204544 | tf_op jit(solution)/shard_map/mul | solution.py:377
  86.4 4.3 %copy.19 = bf16[512,4,512]{0,2,1:T(8,128)(2,1)} copy(bf16[512,4,512]{2,0,1:T(8,128)(2,1)} %fusion.9) | data formatting | bytes 4194304 | tf_op jit(solution)/shard_map/mul | solution.py:377
  90.7 2.9 %convolution_convert_fusion = bf16[512,512]{0,1:T(8,128)(2,1)S(1)} fusion(bf16[512,2048]{0,1:T(8,128)(2,1)} %bitcast.103, bf16[2048,512]{1,0:T(8,128)(2,1)S(1)} %bitcast.97), kind=kOutput, calls=%fused_computation.24 | convolution fusion | flops 1074003968 | bytes 4718592 | tf_op jit(solution)/shard_map/dot_general | solution.py:384
  93.6 0.1 convert.42
  93.8 0.2 subtract_convert_fusion.1
  94.0 0.3 fusion.27
  94.3 0.3 fusion.29
  94.7 0.1 max.38
  94.8 0.1 convert_add_fusion
  94.9 0.1 maximum_maximum_fusion
  95.0 0.8 fusion.7
  95.9 0.1 broadcast_maximum_fusion.1
  95.9 0.9 fusion.5
  96.8 0.8 fusion.8
  97.6 0.1 exponential_add_fusion.1
  97.7 0.9 fusion.6
  98.6 0.1 exponential_add_fusion
  98.7 1.2 fusion.13
  99.9 1.2 fusion.12
  101.2 1.9 %convolution_convert_fusion.1 = bf16[512,256]{0,1:T(8,128)(2,1)S(1)} fusion(bf16[512,256]{0,1:T(8,128)(2,1)S(1)} %convolution_convert_fusion.2, bf16[640,512]{0,1:T(8,128)(2,1)S(1)} %get-tuple-element.42, bf16[640,512]{0,1:T(8,128)(2,1)S(1)} %get-tuple-element.41, f32[512]{0:T(512)S(1)} %get-tuple-element.12, pred[512]{0:T(512)(128)(4,1)S(1)} %get-tuple-element.28, ...), kind=kOutput, calls=%fused_computation.27 | convolution fusion | flops 73793536 | bytes 4597760 | tf_op jit(solution)/shard_map/dot_general | solution.py:399
  103.1 1.3 fusion.32
  104.4 0.1 copy-done.2
  104.5 1.3 add_convert_fusion
  105.8 1.5 %copy.31 = bf16[64,4,8,512]{3,2,0,1:T(8,128)(2,1)} copy(bf16[64,4,8,512]{3,2,1,0:T(8,128)(2,1)S(1)} %bitcast.102) | data formatting | bytes 4194304 | tf_op jit(solution)/shard_map/reshape | solution.py:40
  107.3 4.1 %all-to-all-start = ((bf16[4,512,512]{2,1,0:T(8,128)(2,1)}), bf16[4,512,512]{2,1,0:T(8,128)(2,1)S(1)}, u32[]{:S(2)}, u32[]{:S(2)}) async-start(bf16[4,512,512]{2,1,0:T(8,128)(2,1)} %bitcast.101), calls=%async_computation | async-start | bytes 4194304 | tf_op jit(solution)/shard_map/all_to_all | solution.py:46
  111.5 0.1 log_add_fusion.1
  111.6 0.6 pad_maximum_fusion.12
  112.2 26.0 %all-to-all-done = bf16[4,512,512]{2,1,0:T(8,128)(2,1)S(1)} async-done(((bf16[4,512,512]{2,1,0:T(8,128)(2,1)}), bf16[4,512,512]{2,1,0:T(8,128)(2,1)S(1)}, u32[]{:S(2)}, u32[]{:S(2)}) %all-to-all-start) | async-done | bytes 2097184 | tf_op jit(solution)/shard_map/all_to_all | solution.py:46
  138.2 1.2 reduce_sum.46
  (49 shorter events, 0.4 us)
Async XLA Ops:
  0.6 100.6 %copy-start = (bf16[1,256,256]{2,1,0:T(8,128)(2,1)S(1)}, bf16[1,256,256]{2,1,0:T(8,128)(2,1)}, u32[]{:S(2)}) copy-start(bf16[1,256,256]{2,1,0:T(8,128)(2,1)} %param.16) | copy-start | bytes 393220
  1.4 1.0 copy-start.5
  2.5 0.7 copy-start.6
  3.2 0.7 copy-start.7
  3.9 0.7 copy-start.8
  4.6 0.7 copy-start.9
  65.4 3.6 %copy-start.1 = (bf16[8,8,2,16,384]{4,3,2,1,0:T(8,128)(2,1)}, bf16[8,8,2,16,384]{4,3,2,1,0:T(8,128)(2,1)S(1)}, u32[]{:S(2)}) copy-start(bf16[8,8,2,16,384]{4,3,2,1,0:T(8,128)(2,1)S(1)} %get-tuple-element.11) | copy-start | bytes 4718596
  65.5 3.5 %copy-start.3 = (bf16[8,8,2,16,384]{4,3,2,1,0:T(8,128)(2,1)}, bf16[8,8,2,16,384]{4,3,2,1,0:T(8,128)(2,1)S(1)}, u32[]{:S(2)}) copy-start(bf16[8,8,2,16,384]{4,3,2,1,0:T(8,128)(2,1)S(1)} %get-tuple-element.10) | copy-start | bytes 4718596
  65.5 3.6 %copy-start.10 = (bf16[8,8,2,16,512]{4,3,2,1,0:T(8,128)(2,1)}, bf16[8,8,2,16,512]{4,3,2,1,0:T(8,128)(2,1)S(1)}, u32[]{:S(2)}) copy-start(bf16[8,8,2,16,512]{4,3,2,1,0:T(8,128)(2,1)S(1)} %get-tuple-element.9) | copy-start | bytes 6291460
  65.5 4.1 %copy-start.12 = (bf16[8,8,2,16,512]{4,3,2,1,0:T(8,128)(2,1)}, bf16[8,8,2,16,512]{4,3,2,1,0:T(8,128)(2,1)S(1)}, u32[]{:S(2)}) copy-start(bf16[8,8,2,16,512]{4,3,2,1,0:T(8,128)(2,1)S(1)} %get-tuple-element.8) | copy-start | bytes 6291460
  69.6 5.3 %copy-start.14 = (f32[2048]{0:T(1024)S(1)}, f32[2048]{0:T(1024)}, u32[]{:S(2)}) copy-start(f32[2048]{0:T(1024)} %param.11) | copy-start | bytes 24580
  74.9 2.9 %copy-start.13 = (bf16[8,8,2,16,512]{4,3,2,1,0:T(8,128)(2,1)S(1)}, bf16[8,8,2,16,512]{4,3,2,1,0:T(8,128)(2,1)}, u32[]{:S(2)}) copy-start(bf16[8,8,2,16,512]{4,3,2,1,0:T(8,128)(2,1)} %copy-done.12) | copy-start | bytes 6291460
  80.0 14.8 %collective-permute-start = (bf16[128,512]{0,1:T(8,128)(2,1)S(1)}, bf16[128,512]{0,1:T(8,128)(2,1)S(1)}, u32[]{:S(2)}, u32[]{:S(2)}) collective-permute-start(bf16[128,512]{0,1:T(8,128)(2,1)S(1)} %get-tuple-element.43), channel_id=1, source_target_pairs={{0,4},{4,8},{8,12},{12,16},{16,20},{20,24},{24,28},{28,32},{32,36}... | collective-permute-start | bytes 393224 | tf_op jit(solution)/shard_map/ppermute | solution.py:29
  82.5 12.3 %collective-permute-start.1 = (bf16[128,512]{0,1:T(8,128)(2,1)S(1)}, bf16[128,512]{0,1:T(8,128)(2,1)S(1)}, u32[]{:S(2)}, u32[]{:S(2)}) collective-permute-start(bf16[128,512]{0,1:T(8,128)(2,1)S(1)} %get-tuple-element.44), channel_id=1, source_target_pairs={{4,0},{8,4},{12,8},{16,12},{20,16},{24,20},{28,24},{32,28},{36,32}... | collective-permute-start | bytes 393224 | tf_op jit(solution)/shard_map/ppermute | solution.py:31
  86.4 4.3 %copy-start.11 = (bf16[8,8,2,16,512]{4,3,2,1,0:T(8,128)(2,1)S(1)}, bf16[8,8,2,16,512]{4,3,2,1,0:T(8,128)(2,1)}, u32[]{:S(2)}) copy-start(bf16[8,8,2,16,512]{4,3,2,1,0:T(8,128)(2,1)} %copy-done.10) | copy-start | bytes 6291460
  93.6 1.1 copy-start.15
  101.2 1.9 %copy-start.4 = (bf16[8,8,2,16,384]{4,3,2,1,0:T(8,128)(2,1)S(1)}, bf16[8,8,2,16,384]{4,3,2,1,0:T(8,128)(2,1)}, u32[]{:S(2)}) copy-start(bf16[8,8,2,16,384]{4,3,2,1,0:T(8,128)(2,1)} %copy-done.3) | copy-start | bytes 4718596
  103.1 1.4 %copy-start.2 = (bf16[8,8,2,16,384]{4,3,2,1,0:T(8,128)(2,1)S(1)}, bf16[8,8,2,16,384]{4,3,2,1,0:T(8,128)(2,1)}, u32[]{:S(2)}) copy-start(bf16[8,8,2,16,384]{4,3,2,1,0:T(8,128)(2,1)} %copy-done.1) | copy-start | bytes 4718596
  107.3 30.9 %all-to-all-start = ((bf16[4,512,512]{2,1,0:T(8,128)(2,1)}), bf16[4,512,512]{2,1,0:T(8,128)(2,1)S(1)}, u32[]{:S(2)}, u32[]{:S(2)}) async-start(bf16[4,512,512]{2,1,0:T(8,128)(2,1)} %bitcast.101), calls=%async_computation | async-start | bytes 4194304 | tf_op jit(solution)/shard_map/all_to_all | solution.py:46

commit v2 on v1

v2 whole, which is shorter than its diff:
```python
import jax
import jax.numpy as jnp
from jax import lax
from jax.sharding import Mesh
from jax.experimental import pallas as pl
from jax.experimental.pallas import tpu as pltpu
from jax.sharding import PartitionSpec as P

HD = 64
GRID_W = 64
SP = ("sp_0", "sp_1", "sp_2")


norm_eps = 1e-06
rope_base = 10000.0
neg_fill = -1e30


def rope_tables(positions, head_dim):
    n_freq = head_dim // 4
    freqs = rope_base ** (-jnp.arange(n_freq, dtype=jnp.float32) / n_freq)
    rows = (positions // GRID_W).astype(jnp.float32)
    columns = (positions % GRID_W).astype(jnp.float32)
    row_angle = rows[:, None] * freqs[None, :]
    col_angle = columns[:, None] * freqs[None, :]
    return (jnp.cos(row_angle), jnp.sin(row_angle), jnp.cos(col_angle), jnp.sin(col_angle))


MESH = pl.DeviceIdType.MESH
AX_Z, AX_Y, AX_C, AX_X = "sp_0", "sp_1", "sp_2", "tp"
BLOCK = 128
EDGE = 16


def remote(src, dst, send_sem, recv_sem, device):
    return pltpu.make_async_remote_copy(
        src_ref=src,
        dst_ref=dst,
        send_sem=send_sem,
        recv_sem=recv_sem,
        device_id=device,
        device_id_type=MESH,
    )


def wait_bytes(ref, sem):
    pltpu.make_async_copy(ref, ref, sem).wait()


class Torus:
    def __init__(self, buf, first, size, sems):
        self.buf, self.first, self.size = buf, first, size
        self.p1_send, self.p1_recv, self.p2_send, self.p2_recv, self.d_send, self.d_recv = sems
        self.z, self.y, self.c = lax.axis_index(AX_Z), lax.axis_index(AX_Y), lax.axis_index(AX_C)
        by_y = first == AX_Y
        self.n1, self.n2 = (buf.shape[1], buf.shape[0]) if by_y else (buf.shape[0], buf.shape[1])
        self.a, self.b = (self.y, self.z) if by_y else (self.z, self.y)
        self.second = AX_Z if by_y else AX_Y
        self.groups = self.n1 // size

    def chunk(self, b, start, size):
        if self.first == AX_Y:
            return self.buf.at[b, pl.ds(start, size), self.c]
        return self.buf.at[pl.ds(start, size), b, self.c]

    def group_id(self, k):
        return lax.rem(lax.div(self.a, self.size) + k, self.groups)

    def hops(self, way, k):
        half = self.n2 // 2
        return half if (way == 0) == (k < self.groups // 2) else half - 1

    def phase1_start(self):
        own = self.buf.at[self.z, self.y, self.c]
        order = sorted(range(1, self.n1), key=lambda d: min(d, self.n1 - d))
        for d in order:
            remote(
                own, own, self.p1_send, self.p1_recv.at[self.group_id(0)],
                {self.first: lax.rem(self.a + d, self.n1)},
            ).start()

    def to_partner(self, ref):
        remote(ref, ref, self.d_send, self.d_recv, {AX_C: 1 - self.c}).start()

    def phase1_group(self, k):
        count = self.size - 1 if k == 0 else self.size
        wait_bytes(self.chunk(self.b, 0, count), self.p1_recv.at[self.group_id(k)])
        for way in range(2):
            self.relay(way, k, 1).start()
        self.to_partner(self.chunk(self.b, self.group_id(k) * self.size, self.size))

    def block(self, way, k, back):
        step = 1 if way == 0 else self.n2 - 1
        origin = lax.rem(self.b + back * (self.n2 - step), self.n2)
        return self.chunk(origin, self.group_id(k) * self.size, self.size)

    def relay(self, way, k, hop):
        step = 1 if way == 0 else self.n2 - 1
        ref = self.block(way, k, hop - 1)
        return remote(
            ref, ref, self.p2_send.at[way, k, hop - 1], self.p2_recv.at[way, k, hop - 1],
            {self.second: lax.rem(self.b + step, self.n2)},
        )

    def level(self, hop, k, way):
        last = self.hops(way, k)
        if hop > last + 1:
            return
        ref = self.block(way, k, hop - 1)
        wait_bytes(ref, self.p2_recv.at[way, k, hop - 2])
        if hop <= last:
            self.relay(way, k, hop).start()
        self.to_partner(ref)

    def arrived(self):
        wait_bytes(self.buf.at[:, :, 1 - self.c], self.d_recv)

    def drain(self):
        wait_bytes(self.buf.at[:, :, self.c], self.d_send)
        wait_bytes(self.chunk(self.b, 0, self.n1 - 1), self.p1_send)
        for k in range(self.groups):
            for way in range(2):
                for hop in range(1, self.hops(way, k) + 1):
                    self.relay(way, k, hop).wait_send()


def torus_sems(n1, n2, size):
    dma = pltpu.SemaphoreType.DMA
    groups, hops = n1 // size, n2 // 2
    return [
        dma(()), dma((groups,)), dma((2, groups, hops)), dma((2, groups, hops)), dma(()), dma(()),
    ]


class Ring:
    def __init__(self, buf, sems):
        self.buf = buf
        self.send, self.recv = sems
        self.n, self.x = buf.shape[0], lax.axis_index(AX_X)
        self.half = buf.shape[1] // 2

    def part(self, x, which):
        return self.buf.at[x, which * self.half : (which + 1) * self.half]

    def copy(self, way, index, x, which):
        step = 1 if way == 0 else self.n - 1
        ref = self.part(x, which)
        return remote(
            ref, ref, self.send.at[way, index], self.recv.at[way, index],
            {AX_X: lax.rem(self.x + step, self.n)},
        )

    def start(self):
        for index in range(2):
            for way in range(2):
                self.copy(way, index, self.x, index if way == 0 else 1 - index).start()

    def forward(self):
        for way in range(2):
            step = 1 if way == 0 else self.n - 1
            behind = lax.rem(self.x + self.n - step, self.n)
            wait_bytes(self.part(behind, way), self.recv.at[way, 0])
            self.copy(way, 2, behind, way).start()

    def arrived(self):
        for way in range(2):
            step = 1 if way == 0 else self.n - 1
            behind = lax.rem(self.x + self.n - step, self.n)
            across = lax.rem(self.x + 2, self.n)
            wait_bytes(self.part(behind, 1 - way), self.recv.at[way, 1])
            wait_bytes(self.part(across, way), self.recv.at[way, 2])

    def drain(self):
        for way in range(2):
            for index in range(3):
                self.copy(way, index, self.x, 0).wait_send()


def sequence_neighbour(step):
    nz, ny, nc = (lax.axis_size(a) for a in (AX_Z, AX_Y, AX_C))
    place = (lax.axis_index(AX_Z) * ny + lax.axis_index(AX_Y)) * nc + lax.axis_index(AX_C)
    place = lax.rem(place + step + nz * ny * nc, nz * ny * nc)
    chip = lax.div(place, nc)
    return {AX_Z: lax.div(chip, ny), AX_Y: lax.rem(chip, ny), AX_C: lax.rem(place, nc)}


def greet_all():
    nz, ny, nx = (lax.axis_size(a) for a in (AX_Z, AX_Y, AX_X))
    z, y, c, x = (lax.axis_index(a) for a in (AX_Z, AX_Y, AX_C, AX_X))
    peers = [sequence_neighbour(1), sequence_neighbour(-1), {AX_C: 1 - c}]
    peers += [{AX_X: lax.rem(x + d, nx)} for d in (1, nx - 1)]
    peers += [{AX_Y: lax.rem(y + d, ny)} for d in range(1, ny)]
    peers += [{AX_Z: lax.rem(z + d, nz)} for d in range(1, nz)]
    barrier = pltpu.get_barrier_semaphore()
    for peer in peers:
        pl.semaphore_signal(barrier, inc=1, device_id=peer, device_id_type=MESH)
    pl.semaphore_wait(barrier, len(peers))


def turned(values, cosine, sine):
    lane = lax.broadcasted_iota(jnp.int32, values.shape, 1)
    ahead = pltpu.roll(values, 112, 1)
    behind = pltpu.roll(values, 16, 1)
    return values * cosine + jnp.where(lax.rem(lane, 32) < 16, ahead, behind) * sine


def rounded(values):
    return values.astype(jnp.bfloat16).astype(jnp.float32)


def rows_of(buf, start, size, columns):
    parts = buf[start // 256 : (start + size) // 256, :, :, :, columns]
    return parts.reshape(size, -1)


def normalise(t_buf, gain_ref, normed):
    def step(i, carry):
        rows = pl.ds(pl.multiple_of(i * BLOCK, BLOCK), BLOCK)
        parts = [t_buf[k, rows, :].astype(jnp.float32) for k in range(4)]
        total = sum(jnp.sum(p * p, axis=-1, keepdims=True) for p in parts)
        scale = lax.rsqrt(total / 2048.0 + norm_eps)
        for k in range(4):
            cols = slice(k * 512, (k + 1) * 512)
            normed[rows, cols] = (parts[k] * scale * gain_ref[0:1, cols]).astype(jnp.bfloat16)
        return carry

    lax.fori_loop(0, 4, step, 0)


def project_keys(normed, wb, cos_ref, sin_ref, kv_ext):
    both = jnp.dot(
        normed[...], rows_of(wb, 0, 2048, slice(0, 256)), preferred_element_type=jnp.float32
    )
    keys = turned(rounded(both[:, :128]), cos_ref[...], sin_ref[...])
    kv_ext[BLOCK : BLOCK + 512, 0:128] = keys.astype(jnp.bfloat16)
    kv_ext[BLOCK : BLOCK + 512, 128:256] = both[:, 128:].astype(jnp.bfloat16)


def project_pool(normed, wb, pool_ext):
    pool_ext[EDGE : EDGE + 512, :] = jnp.dot(
        normed[...], rows_of(wb, 0, 2048, slice(256, 512)), preferred_element_type=jnp.float32
    ).astype(jnp.bfloat16)


def project_queries(normed, wa, cos_ref, sin_ref, queries, h):
    cols = slice(h * 256, (h + 1) * 256)
    found = jnp.dot(normed[...], rows_of(wa, 0, 2048, cols), preferred_element_type=jnp.float32)
    for pair in range(2):
        values = turned(
            rounded(found[:, pair * 128 : (pair + 1) * 128]), cos_ref[...], sin_ref[...]
        ) * (HD**-0.5)
        lane = lax.broadcasted_iota(jnp.int32, values.shape, 1)
        mine = (lane < 64) if h == 0 else (lane >= 64)
        for odd in range(2):
            placed = values if odd == h else pltpu.roll(values, 64, 1)
            placed = jnp.where(mine, placed, 0.0).astype(jnp.bfloat16)
            g = pair * 2 + odd
            for b in range(4):
                queries[h, b, g * BLOCK : (g + 1) * BLOCK, :] = placed[b * BLOCK : (b + 1) * BLOCK]


def attend(b, h, place, places, kv_ext, queries, sink_ref, features, log_ref):
    start = pl.multiple_of(b * BLOCK, BLOCK)
    keys = kv_ext[pl.ds(start, 3 * BLOCK), 0:128]
    scores = lax.dot_general(
        keys, queries[h, b], (((1,), (1,)), ((), ())), preferred_element_type=jnp.float32
    )
    shape = (BLOCK, 4 * BLOCK)
    key = lax.broadcasted_iota(jnp.int32, shape, 0)
    query = lax.rem(lax.broadcasted_iota(jnp.int32, shape, 1), BLOCK)
    first = jnp.where((place == 0) & (b == 0), BLOCK, 0)
    last = jnp.where((place == places - 1) & (b == 3), -1, BLOCK)
    before = jnp.where(key >= jnp.maximum(query, first), scores[:BLOCK], neg_fill)
    here = scores[BLOCK : 2 * BLOCK]
    after = jnp.where(key <= jnp.minimum(query, last), scores[2 * BLOCK :], neg_fill)
    sink = sink_ref[h : h + 1, :]
    top = jnp.max(jnp.maximum(jnp.maximum(before, here), after), axis=0, keepdims=True)
    top = jnp.maximum(top, sink)
    exps = [jnp.exp(part - top) for part in (before, here, after)]
    total = jnp.sum(exps[0] + exps[1] + exps[2], axis=0, keepdims=True) + jnp.exp(sink - top)
    logs = top + jnp.log(total)
    weights = jnp.concatenate([e.astype(jnp.bfloat16) for e in exps], axis=0)
    values = kv_ext[pl.ds(start, 3 * BLOCK), 128:256]
    summed = lax.dot_general(
        values, weights, (((0,), (0,)), ((), ())), preferred_element_type=jnp.float32
    )
    mine = summed[h * 64 : (h + 1) * 64] / total
    for g in range(4):
        log_ref[4 * h + g : 4 * h + g + 1, pl.ds(start, BLOCK)] = logs[
            :, g * BLOCK : (g + 1) * BLOCK
        ]
    for pair in range(2):
        two = jnp.concatenate(
            [mine[:, (2 * pair + e) * BLOCK : (2 * pair + e + 1) * BLOCK] for e in range(2)], axis=0
        )
        at = 256 + h * 256 + pair * 128
        features[pl.ds(start, BLOCK), at : at + 128] = two.T.astype(jnp.bfloat16)


def pool(b, place, places, reach, pool_ext, mix_ref, features):
    start = pl.multiple_of(b * BLOCK, BLOCK)
    size = BLOCK + 2 * EDGE
    base = place * 512 + b * BLOCK
    row = lax.broadcasted_iota(jnp.int32, (BLOCK, size), 0)
    col = lax.broadcasted_iota(jnp.int32, (BLOCK, size), 1) - EDGE
    inside = (col >= row - reach) & (col < row + reach)
    inside = inside & (col >= -base) & (col < places * 512 - base)
    band = jnp.where(inside, 1.0, 0.0)
    counted = jnp.sum(band, axis=-1, keepdims=True)
    ext = pool_ext[pl.ds(start, size), :]
    summed = jnp.dot(band.astype(jnp.bfloat16), ext, preferred_element_type=jnp.float32)
    own = ext[EDGE : EDGE + BLOCK].astype(jnp.float32)
    pooled = (summed / counted - own).astype(jnp.bfloat16)
    features[pl.ds(start, BLOCK), 0:256] = jnp.dot(
        pooled, mix_ref[0], preferred_element_type=jnp.float32
    ).astype(jnp.bfloat16)


def partial_term(b, j, features, oa, ob):
    rows = pl.ds(pl.multiple_of(b * BLOCK, BLOCK), BLOCK)
    dims = (((1,), (1,)), ((), ()))
    low = oa[pl.ds(2 * j, 2)].reshape(512, 384)
    high = ob[pl.ds(2 * j, 2)].reshape(512, 384)
    return lax.dot_general(
        features[rows, 0:384], low, dims, preferred_element_type=jnp.float32
    ) + lax.dot_general(features[rows, 384:768], high, dims, preferred_element_type=jnp.float32)


class Scatter:
    def __init__(self, refs, sems):
        self.far, self.near, self.far_in, self.near_in, self.kept = refs
        self.far_send, self.far_recv, self.near_send, self.near_recv = sems
        self.n, self.x = lax.axis_size(AX_X), lax.axis_index(AX_X)
        self.half = BLOCK // 2

    def target(self, way):
        return lax.rem(self.x + (1 if way == 0 else self.n - 1), self.n)

    def far_copy(self, b, way):
        rows = slice(way * self.half, (way + 1) * self.half)
        return remote(
            self.far.at[b, rows], self.far_in.at[b, way],
            self.far_send.at[b, way], self.far_recv.at[b, way], {AX_X: self.target(way)},
        )

    def near_copy(self, b, way, added):
        which = way if added else 1 - way
        rows = slice(which * self.half, (which + 1) * self.half)
        index = 1 if added else 0
        return remote(
            self.near.at[b, way, rows], self.near_in.at[b, way, rows],
            self.near_send.at[b, way, index], self.near_recv.at[b, way, index],
            {AX_X: self.target(way)},
        )

    def compute(self, b, features, oa, ob):
        across = lax.rem(self.x + 2, self.n)
        self.far[b] = partial_term(b, across, features, oa, ob).astype(jnp.bfloat16)
        for way in range(2):
            self.near[b, way] = partial_term(b, self.target(way), features, oa, ob).astype(jnp.bfloat16)
            self.far_copy(b, way).start()
        self.kept[b] = partial_term(b, self.x, features, oa, ob).astype(jnp.bfloat16)
        for way in range(2):
            self.near_copy(b, way, False).start()

    def add(self, b):
        for way in range(2):
            rows = slice(way * self.half, (way + 1) * self.half)
            self.far_copy(b, way).wait_recv()
            both = self.near[b, way, rows].astype(jnp.float32) + self.far_in[b, way].astype(jnp.float32)
            self.near[b, way, rows] = both.astype(jnp.bfloat16)
        for way in range(2):
            self.near_copy(b, way, True).start()

    def finish(self, b, out_ref):
        for way in range(2):
            for added in (False, True):
                self.near_copy(b, way, added).wait_recv()
        total = self.kept[b].astype(jnp.float32)
        for way in range(2):
            total = total + self.near_in[b, way].astype(jnp.float32)
        out_ref[pl.ds(pl.multiple_of(b * BLOCK, BLOCK), BLOCK), :] = total.astype(jnp.bfloat16)

    def drain(self, b):
        for way in range(2):
            self.far_copy(b, way).wait_send()
            for added in (False, True):
                self.near_copy(b, way, added).wait_send()


def layer_kernel(
    tok_ref, q_ref, k_ref, v_ref, p_ref, oa_ref, ob_ref,
    gain_ref, mix_ref, sink_ref, cos_ref, sin_ref,
    out_ref, log_ref,
    t_buf, wa, wb, oa, ob, normed, queries, kv_ext, pool_ext, features,
    far, near, far_in, near_in, kept,
    load_sem, ring_send, ring_recv, halo_send, halo_recv, far_send, far_recv, near_send, near_recv,
    *torus,
):
    z, y, c, x = (lax.axis_index(a) for a in (AX_Z, AX_Y, AX_C, AX_X))
    nz, ny, nc = (lax.axis_size(a) for a in (AX_Z, AX_Y, AX_C))
    place, places = (z * ny + y) * nc + c, nz * ny * nc
    ring = Ring(t_buf, (ring_send, ring_recv))
    ins = [Torus(wa, AX_Y, 2, torus[0:6]), Torus(wb, AX_Z, 2, torus[6:12])]
    outs = [Torus(oa, AX_Y, 4, torus[12:18]), Torus(ob, AX_Z, 4, torus[18:24])]
    loads = [
        pltpu.make_async_copy(tok_ref, t_buf.at[x], load_sem.at[0]),
        pltpu.make_async_copy(q_ref, wa.at[z, y, c], load_sem.at[1]),
        pltpu.make_async_copy(k_ref, wb.at[z, y, c, :, 0:128], load_sem.at[2]),
        pltpu.make_async_copy(v_ref, wb.at[z, y, c, :, 128:256], load_sem.at[3]),
        pltpu.make_async_copy(p_ref, wb.at[z, y, c, :, 256:512], load_sem.at[4]),
        pltpu.make_async_copy(oa_ref, oa.at[z, y, c], load_sem.at[5]),
        pltpu.make_async_copy(ob_ref, ob.at[z, y, c], load_sem.at[6]),
    ]
    for load in loads:
        load.start()
    greet_all()
    for load in loads:
        load.wait()
    for t in ins:
        t.phase1_start()
    ring.start()
    for k in range(ins[0].groups):
        for t in ins:
            t.phase1_group(k)

    def levels(group, hop):
        for k in range(group[0].groups):
            for way in range(2):
                for t in group:
                    t.level(hop, k, way)

    levels(ins, 2)
    ring.forward()
    levels(ins, 3)
    levels(ins, 4)
    for t in outs:
        t.phase1_start()
    levels(ins, 5)
    ring.arrived()
    normalise(t_buf, gain_ref, normed)
    for k in range(outs[0].groups):
        for t in outs:
            t.phase1_group(k)
    for t in ins:
        t.arrived()

    project_keys(normed, wb, cos_ref, sin_ref, kv_ext)
    project_pool(normed, wb, pool_ext)

    def halo_copies(way):
        low = 512 if way == 0 else BLOCK
        high = 0 if way == 0 else BLOCK + 512
        plow = 512 if way == 0 else EDGE
        phigh = 0 if way == 0 else EDGE + 512
        device = sequence_neighbour(1 if way == 0 else -1)
        return [
            remote(
                kv_ext.at[low : low + BLOCK], kv_ext.at[high : high + BLOCK],
                halo_send.at[way, 0], halo_recv.at[way, 0], device,
            ),
            remote(
                pool_ext.at[plow : plow + EDGE], pool_ext.at[phigh : phigh + EDGE],
                halo_send.at[way, 1], halo_recv.at[way, 1], device,
            ),
        ]

    for way in range(2):
        for copy in halo_copies(way):
            copy.start()
    levels(outs, 2)
    for h in range(2):
        project_queries(normed, wa, cos_ref, sin_ref, queries, h)
    levels(outs, 3)
    reach = lax.shift_left(jnp.int32(1), x)

    def block(i, carry):
        b = i + 1 - 4 * lax.div(i, 3)
        for h in range(2):
            attend(b, h, place, places, kv_ext, queries, sink_ref, features, log_ref)
        pool(b, place, places, reach, pool_ext, mix_ref, features)
        return carry

    lax.fori_loop(0, 2, block, 0)
    levels(outs, 4)
    for way in range(2):
        for copy in halo_copies(way):
            copy.wait_recv()
    lax.fori_loop(2, 4, block, 0)
    levels(outs, 5)
    for t in outs:
        t.arrived()

    scatter = Scatter(
        (far, near, far_in, near_in, kept), (far_send, far_recv, near_send, near_recv)
    )

    def send(b, carry):
        scatter.compute(b, features, oa, ob)

        @pl.when(b > 0)
        def _():
            scatter.add(b - 1)

        return carry

    lax.fori_loop(0, 4, send, 0)
    scatter.add(3)

    def close(b, carry):
        scatter.finish(b, out_ref)
        scatter.drain(b)
        return carry

    lax.fori_loop(0, 4, close, 0)
    for t in ins + outs:
        t.drain()
    ring.drain()
    for way in range(2):
        for copy in halo_copies(way):
            copy.wait_send()


def whole_layer(tokens, weights, out_a, out_b, gain, mix, sink, cosine, sine):
    nz, ny, nc, nx = (lax.axis_size(a) for a in (AX_Z, AX_Y, AX_C, AX_X))
    rows, width = tokens.shape
    bf = jnp.bfloat16
    dma = pltpu.SemaphoreType.DMA
    vmem = pltpu.VMEM
    blocks = rows // BLOCK
    near_data = pl.BlockSpec(memory_space=pltpu.VMEM)
    return pl.pallas_call(
        layer_kernel,
        out_shape=[
            jax.ShapeDtypeStruct((rows, width), bf),
            jax.ShapeDtypeStruct((8, rows), jnp.float32),
        ],
        in_specs=[pl.BlockSpec(memory_space=pltpu.HBM)] * 7 + [near_data] * 5,
        out_specs=[near_data] * 2,
        scratch_shapes=[
            vmem((nx, rows, width), bf),
            vmem((nz, ny, nc, 16, 512), bf),
            vmem((nz, ny, nc, 16, 512), bf),
            vmem((nz, ny, nc, 16, 384), bf),
            vmem((nz, ny, nc, 16, 384), bf),
            vmem((rows, nx * width), bf),
            vmem((2, blocks, 4 * BLOCK, 128), bf),
            vmem((rows + 2 * BLOCK, 256), bf),
            vmem((rows + 2 * EDGE, 256), bf),
            vmem((rows, 768), bf),
            vmem((blocks, BLOCK, 512), bf),
            vmem((blocks, 2, BLOCK, 512), bf),
            vmem((blocks, 2, BLOCK // 2, 512), bf),
            vmem((blocks, 2, BLOCK, 512), bf),
            vmem((blocks, BLOCK, 512), bf),
            dma((7,)), dma((2, 3)), dma((2, 3)), dma((2, 2)), dma((2, 2)),
            dma((blocks, 2)), dma((blocks, 2)), dma((blocks, 2, 2)), dma((blocks, 2, 2)),
        ]
        + torus_sems(ny, nz, 2) + torus_sems(nz, ny, 2) + torus_sems(ny, nz, 4) + torus_sems(nz, ny, 4),
        compiler_params=pltpu.CompilerParams(
            collective_id=0, has_side_effects=True, vmem_limit_bytes=56 * 1024 * 1024
        ),
    )(tokens, *weights, out_a, out_b, gain, mix, sink, cosine, sine)


def local(
    tokens,
    norm_gain,
    query_weight,
    key_weight,
    value_weight,
    pool_in_weight,
    pool_mix_weight,
    sink_logit,
    out_pool_weight,
    out_attn_weight,
):
    rows = tokens.shape[0]
    positions = lax.axis_index(SP) * rows + jnp.arange(rows, dtype=jnp.int32)
    cos_r, sin_r, cos_c, sin_c = rope_tables(positions, HD)
    cosine = jnp.concatenate([cos_r, cos_r, cos_c, cos_c] * 2, 1)
    sine = jnp.concatenate([-sin_r, sin_r, -sin_c, sin_c] * 2, 1)
    out_rows = jnp.concatenate([out_pool_weight, out_attn_weight], 0).T
    mixed, log_weight = whole_layer(
        tokens,
        (query_weight, key_weight, value_weight, pool_in_weight),
        out_rows[:, :384],
        out_rows[:, 384:],
        norm_gain[None],
        pool_mix_weight,
        jnp.repeat(sink_logit, BLOCK).reshape(2, 4 * BLOCK),
        cosine,
        sine,
    )
    return (mixed, log_weight)


def solution(mesh):
    finer = Mesh(mesh.devices.reshape(8, 8, 2, mesh.shape["tp"]), ("sp_0", "sp_1", "sp_2", "tp"))
    placed = (
        P(SP, "tp"),
        P(),
        P(SP, "tp"),
        P(SP, "tp"),
        P(SP, "tp"),
        P(SP, "tp"),
        P("tp", None, None),
        P("tp"),
        P("tp", SP),
        P("tp", SP),
    )
    return jax.shard_map(
        local, mesh=finer, in_specs=placed, out_specs=(P(SP, "tp"), P("tp", SP)), check_vma=False
    )
```

time: 140 us -> 90.4 us (0.65)
  waiting for transfers between devices: 26 us -> 0 us
  Pallas kernels: 60.2 us -> 80.3 us
  matrix products: 13.2 us -> 0 us
  other arithmetic: 14.3 us -> 1.93 us
  local copies, waits for them, and re-layouts: 16 us -> 7.35 us
  starting transfers between devices: 8.53 us -> 0 us
    all_to_all x1 -> x0, waiting for transfers between devices: 26 us -> none  [summed_on_arrival(): lax.all_to_all(in_blocks(shard, dim, count), axis, 0, 0, tiled=True)]
    pallas_call x1, Pallas kernels: 60.2 us -> 80.3 us  [whole_layer(): pl.pallas_call(layer_kernel, out_shape=[jax.ShapeDtypeStruct((rows, width...]
    dot_general x11 -> x0, matrix products: 13.2 us -> none  [the longest x4 4.62 us: local(): jnp.dot(normed, piece, preferred_element_type=jnp.float32)]
    convert_element_type x2 -> x0, other arithmetic: 5.79 us -> none  [the longest x1 3.02 us: local(): wide = whole.astype(jnp.float32)]
    convert_element_type x1 -> x0, local copies, waits for them, and re-layouts: 5.31 us -> none  [local(): wide = whole.astype(jnp.float32)]
    ppermute x2 -> x0, starting transfers between devices: 4.45 us -> none  [the longest x1 2.53 us: with_halo(): lax.ppermute(tail, axis, [(i, (i + 1) % count) for i in range(ends)])]
    mul x2 -> x0, local copies, waits for them, and re-layouts: 4.32 us -> none  [local(): wide * lax.rsqrt(jnp.mean(wide * wide, -1, keepdims=True) + norm_eps)]
    all_to_all x1 -> x0, starting transfers between devices: 4.09 us -> none  [summed_on_arrival(): lax.all_to_all(in_blocks(shard, dim, count), axis, 0, 0, tiled=True)]
  transfers between devices with their start and end apart: 3 -> 0, of which waited for: 1 -> 0; matrix products, arithmetic and copies ran while one was open for 8% -> 0% of each run, Pallas kernels for 0% -> 0%
where the time goes in v2:
time: 90.4 us; the launch traced here: 90.2 us
  Pallas kernels  80.3 us (89%)
  local copies, waits for them, and re-layouts  7.35 us (8%)
  other arithmetic  1.93 us (2%)
    pallas_call x1, Pallas kernels, whole_layer(): pl.pallas_call(layer_kernel, out_shape=[jax.ShapeDtypeStruct((rows, width...  80.3 us
    unnamed x12, local copies, waits for them, and re-layouts  3.82 us
    sin x1, other arithmetic, rope_tables(): jnp.sin(col_angle)  1.9 us

profile of v2, /device:TPU:1, one launch (start us, length us, event | category | flops | bytes accessed | tf_op | source)
XLA Modules:
  0.0 90.2 jit_solution(13317044878022652705)
XLA Ops:
  0.7 1.9 %multiply_sine_fusion = (f32[512,16]{1,0:T(8,128)S(1)}, f32[512,16]{1,0:T(8,128)S(1)}, f32[512,16]{1,0:T(8,128)S(1)}, f32[512,16]{1,0:T(8,128)S(1)}, f32[512,16]{1,0:T(8,128)S(1)}, /*index=5*/f32[512,16]{1,0:T(8,128)S(1)}) fusion(f32[512]{0:T(512)S(1)} %get-tuple-element.14, f32[16]{0:T(128)S(1)} %multiply_power_fusion, f32[512]{0:T(512)S(1)} %get-tuple-element.13), kind=kLoop, calls=%fused_computation | loop fusion | flops 32768 | bytes 200768 | tf_op jit(solution)/shard_map/sin | solution.py:26
  2.6 1.4 %concatenate.11.sin_ref = f32[512,128]{1,0:T(8,128)} concatenate(f32[512,16]{1,0:T(8,128)S(1)} %get-tuple-element.11, f32[512,16]{1,0:T(8,128)S(1)} %get-tuple-element.12, f32[512,16]{1,0:T(8,128)S(1)} %get-tuple-element.5, f32[512,16]{1,0:T(8,128)S(1)} %get-tuple-element.4, f32[512,16]{1,0:T(8,128)S(1)} %get-tuple-element.11, f32[512,16]{1,0:T(8,128)S(1)} %get-tuple-element.12, ...), dimensions={1} | concatenate | bytes 524288 | tf_op jit(solution)/shard_map/concatenate | solution.py:582
  4.0 0.0 copy-start
  4.0 0.0 copy-start.2
  4.0 1.4 %concatenate.10.cos_ref = f32[512,128]{1,0:T(8,128)} concatenate(f32[512,16]{1,0:T(8,128)S(1)} %get-tuple-element.10, f32[512,16]{1,0:T(8,128)S(1)} %get-tuple-element.10, f32[512,16]{1,0:T(8,128)S(1)} %get-tuple-element.6, f32[512,16]{1,0:T(8,128)S(1)} %get-tuple-element.6, f32[512,16]{1,0:T(8,128)S(1)} %get-tuple-element.10, f32[512,16]{1,0:T(8,128)S(1)} %get-tuple-element.10, ...), dimensions={1} | concatenate | bytes 524288 | tf_op jit(solution)/shard_map/concatenate | solution.py:581
  5.4 0.0 copy-done
  5.4 0.0 copy-done.2
  5.4 0.6 fusion.7
  6.0 0.0 copy-start.3
  6.1 0.7 copy-done.3
  6.7 0.1 broadcast_in_dim.15
  6.8 0.1 broadcast_bitcast_fusion
  6.9 0.6 copy.16
  7.5 80.3 %shard_map.113 = (bf16[512,512]{1,0:T(8,128)(2,1)}, f32[8,512]{1,0:T(8,128)}) custom-call(bf16[512,512]{1,0:T(8,128)(2,1)} %tok_ref.1, bf16[16,512]{1,0:T(8,128)(2,1)} %q_ref.1, bf16[16,128]{1,0:T(8,128)(2,1)} %k_ref.1, bf16[16,128]{1,0:T(8,128)(2,1)} %v_ref.1, bf16[16,256]{1,0:T(8,128)(2,1)} %p_ref.1, bf16[16,384]{1,0:T(8,128)(2,1)} %get-tuple-element.3.oa_ref, ...), custom_call_target="tpu_custom_call" | custom-call | tf_op jit(solution)/shard_map/pallas_call | solution.py:532
  87.7 0.0 copy-start.1
  87.7 1.9 %copy.19 = bf16[512,512]{1,0:T(8,128)(2,1)} copy(bf16[512,512]{1,0:T(8,128)(2,1)} %get-tuple-element.17) | data formatting | bytes 1048576
  89.6 0.0 copy-done.1
  89.6 0.6 copy.20
  (3 shorter events, 0.0 us)
Async XLA Ops:
  4.0 1.4 %copy-start = (bf16[512,16]{0,1:T(8,128)(2,1)S(1)}, bf16[512,16]{0,1:T(8,128)(2,1)}, u32[]{:S(2)}) copy-start(bf16[512,16]{0,1:T(8,128)(2,1)} %param.19) | copy-start | bytes 49156
  4.0 1.4 %copy-start.2 = (bf16[256,16]{0,1:T(8,128)(2,1)S(1)}, bf16[256,16]{0,1:T(8,128)(2,1)}, u32[]{:S(2)}) copy-start(bf16[256,16]{0,1:T(8,128)(2,1)} %param.18) | copy-start | bytes 24580
  6.0 0.7 copy-start.3
  87.7 1.9 %copy-start.1 = (f32[8,512]{1,0:T(8,128)S(1)}, f32[8,512]{1,0:T(8,128)}, u32[]{:S(2)}) copy-start(f32[8,512]{1,0:T(8,128)} %get-tuple-element.18) | copy-start | bytes 49156

commit v3 on v2

--- a/solution.py
+++ b/solution.py
@@ -1,5 +1,6 @@
 import jax
 import jax.numpy as jnp
+import numpy as np
 from jax import lax
 from jax.sharding import Mesh
 from jax.experimental import pallas as pl
@@ -14,16 +15,6 @@
 norm_eps = 1e-06
 rope_base = 10000.0
 neg_fill = -1e30
-
-
-def rope_tables(positions, head_dim):
-    n_freq = head_dim // 4
-    freqs = rope_base ** (-jnp.arange(n_freq, dtype=jnp.float32) / n_freq)
-    rows = (positions // GRID_W).astype(jnp.float32)
-    columns = (positions % GRID_W).astype(jnp.float32)
-    row_angle = rows[:, None] * freqs[None, :]
-    col_angle = columns[:, None] * freqs[None, :]
-    return (jnp.cos(row_angle), jnp.sin(row_angle), jnp.cos(col_angle), jnp.sin(col_angle))
 
 
 MESH = pl.DeviceIdType.MESH
@@ -206,6 +197,20 @@
 
 def rounded(values):
     return values.astype(jnp.bfloat16).astype(jnp.float32)
+
+
+def fill_tables(place, freq_ref, cos_buf, sin_buf):
+    row = (lax.broadcasted_iota(jnp.int32, (8, 128), 0) + place * 8).astype(jnp.float32)
+    row_cos, row_sin = jnp.cos(row * freq_ref[0:1]), jnp.sin(row * freq_ref[0:1])
+    col = lax.broadcasted_iota(jnp.int32, (GRID_W, 128), 0).astype(jnp.float32)
+    col_cos, col_sin = jnp.cos(col * freq_ref[0:1]), jnp.sin(col * freq_ref[0:1])
+    lane = lax.broadcasted_iota(jnp.int32, (GRID_W, 128), 1)
+    by_row = lax.rem(lane, 64) < 32
+    sign = jnp.where(lax.rem(lane, 32) < 16, -1.0, 1.0)
+    for r in range(8):
+        rows = slice(r * GRID_W, (r + 1) * GRID_W)
+        cos_buf[rows] = jnp.where(by_row, row_cos[r : r + 1], col_cos)
+        sin_buf[rows] = jnp.where(by_row, row_sin[r : r + 1], col_sin) * sign
 
 
 def rows_of(buf, start, size, columns):
@@ -273,7 +278,7 @@
     before = jnp.where(key >= jnp.maximum(query, first), scores[:BLOCK], neg_fill)
     here = scores[BLOCK : 2 * BLOCK]
     after = jnp.where(key <= jnp.minimum(query, last), scores[2 * BLOCK :], neg_fill)
-    sink = sink_ref[h : h + 1, :]
+    sink = jnp.concatenate([jnp.full((1, BLOCK), sink_ref[4 * h + g], jnp.float32) for g in range(4)], 1)
     top = jnp.max(jnp.maximum(jnp.maximum(before, here), after), axis=0, keepdims=True)
     top = jnp.maximum(top, sink)
     exps = [jnp.exp(part - top) for part in (before, here, after)]
@@ -389,10 +394,10 @@
 
 
 def layer_kernel(
-    tok_ref, q_ref, k_ref, v_ref, p_ref, oa_ref, ob_ref,
-    gain_ref, mix_ref, sink_ref, cos_ref, sin_ref,
+    tok_ref, q_ref, k_ref, v_ref, p_ref, op_ref, oq_ref,
+    gain_ref, mix_ref, freq_ref, sink_ref,
     out_ref, log_ref,
-    t_buf, wa, wb, oa, ob, normed, queries, kv_ext, pool_ext, features,
+    t_buf, wa, wb, oa, ob, cos_ref, sin_ref, normed, queries, kv_ext, pool_ext, features,
     far, near, far_in, near_in, kept,
     load_sem, ring_send, ring_recv, halo_send, halo_recv, far_send, far_recv, near_send, near_recv,
     *torus,
@@ -409,8 +414,9 @@
         pltpu.make_async_copy(k_ref, wb.at[z, y, c, :, 0:128], load_sem.at[2]),
         pltpu.make_async_copy(v_ref, wb.at[z, y, c, :, 128:256], load_sem.at[3]),
         pltpu.make_async_copy(p_ref, wb.at[z, y, c, :, 256:512], load_sem.at[4]),
-        pltpu.make_async_copy(oa_ref, oa.at[z, y, c], load_sem.at[5]),
-        pltpu.make_async_copy(ob_ref, ob.at[z, y, c], load_sem.at[6]),
+        pltpu.make_async_copy(op_ref, oa.at[z, y, c, :, 0:256], load_sem.at[5]),
+        pltpu.make_async_copy(oq_ref.at[:, 0:128], oa.at[z, y, c, :, 256:384], load_sem.at[6]),
+        pltpu.make_async_copy(oq_ref.at[:, 128:512], ob.at[z, y, c], load_sem.at[7]),
     ]
     for load in loads:
         load.start()
@@ -420,8 +426,10 @@
     for t in ins:
         t.phase1_start()
     ring.start()
-    for k in range(ins[0].groups):
-        for t in ins:
+    fill_tables(place, freq_ref, cos_ref, sin_ref)
+
+    def first(group, k):
+        for t in group:
             t.phase1_group(k)
 
     def levels(group, hop):
@@ -430,18 +438,21 @@
                 for t in group:
                     t.level(hop, k, way)
 
+    for k in range(ins[0].groups):
+        first(ins, k)
+    for t in outs:
+        t.phase1_start()
     levels(ins, 2)
     ring.forward()
     levels(ins, 3)
+    for k in range(outs[0].groups):
+        first(outs, k)
     levels(ins, 4)
-    for t in outs:
-        t.phase1_start()
+    levels(outs, 2)
     levels(ins, 5)
     ring.arrived()
+    levels(outs, 3)
     normalise(t_buf, gain_ref, normed)
-    for k in range(outs[0].groups):
-        for t in outs:
-            t.phase1_group(k)
     for t in ins:
         t.arrived()
 
@@ -468,46 +479,39 @@
     for way in range(2):
         for copy in halo_copies(way):
             copy.start()
-    levels(outs, 2)
     for h in range(2):
         project_queries(normed, wa, cos_ref, sin_ref, queries, h)
-    levels(outs, 3)
+    levels(outs, 4)
+    levels(outs, 5)
+    for t in outs:
+        t.arrived()
     reach = lax.shift_left(jnp.int32(1), x)
+    scatter = Scatter(
+        (far, near, far_in, near_in, kept), (far_send, far_recv, near_send, near_recv)
+    )
 
     def block(i, carry):
-        b = i + 1 - 4 * lax.div(i, 3)
+        b = lax.rem(i + 1, 4)
         for h in range(2):
             attend(b, h, place, places, kv_ext, queries, sink_ref, features, log_ref)
         pool(b, place, places, reach, pool_ext, mix_ref, features)
+        scatter.compute(b, features, oa, ob)
+
+        @pl.when(i > 0)
+        def _():
+            scatter.add(i)
+
         return carry
 
     lax.fori_loop(0, 2, block, 0)
-    levels(outs, 4)
     for way in range(2):
         for copy in halo_copies(way):
             copy.wait_recv()
     lax.fori_loop(2, 4, block, 0)
-    levels(outs, 5)
-    for t in outs:
-        t.arrived()
-
-    scatter = Scatter(
-        (far, near, far_in, near_in, kept), (far_send, far_recv, near_send, near_recv)
-    )
-
-    def send(b, carry):
-        scatter.compute(b, features, oa, ob)
-
-        @pl.when(b > 0)
-        def _():
-            scatter.add(b - 1)
-
-        return carry
-
-    lax.fori_loop(0, 4, send, 0)
-    scatter.add(3)
-
-    def close(b, carry):
+    scatter.add(0)
+
+    def close(i, carry):
+        b = lax.rem(i + 1, 4)
         scatter.finish(b, out_ref)
         scatter.drain(b)
         return carry
@@ -521,7 +525,7 @@
             copy.wait_send()
 
 
-def whole_layer(tokens, weights, out_a, out_b, gain, mix, sink, cosine, sine):
+def whole_layer(tokens, weights, gain, mix, freq, sink):
     nz, ny, nc, nx = (lax.axis_size(a) for a in (AX_Z, AX_Y, AX_C, AX_X))
     rows, width = tokens.shape
     bf = jnp.bfloat16
@@ -535,7 +539,8 @@
             jax.ShapeDtypeStruct((rows, width), bf),
             jax.ShapeDtypeStruct((8, rows), jnp.float32),
         ],
-        in_specs=[pl.BlockSpec(memory_space=pltpu.HBM)] * 7 + [near_data] * 5,
+        in_specs=[pl.BlockSpec(memory_space=pltpu.HBM)] * 7 + [near_data] * 3
+        + [pl.BlockSpec(memory_space=pltpu.SMEM)],
         out_specs=[near_data] * 2,
         scratch_shapes=[
             vmem((nx, rows, width), bf),
@@ -543,6 +548,8 @@
             vmem((nz, ny, nc, 16, 512), bf),
             vmem((nz, ny, nc, 16, 384), bf),
             vmem((nz, ny, nc, 16, 384), bf),
+            vmem((rows, 128), jnp.float32),
+            vmem((rows, 128), jnp.float32),
             vmem((rows, nx * width), bf),
             vmem((2, blocks, 4 * BLOCK, 128), bf),
             vmem((rows + 2 * BLOCK, 256), bf),
@@ -553,14 +560,14 @@
             vmem((blocks, 2, BLOCK // 2, 512), bf),
             vmem((blocks, 2, BLOCK, 512), bf),
             vmem((blocks, BLOCK, 512), bf),
-            dma((7,)), dma((2, 3)), dma((2, 3)), dma((2, 2)), dma((2, 2)),
+            dma((8,)), dma((2, 3)), dma((2, 3)), dma((2, 2)), dma((2, 2)),
             dma((blocks, 2)), dma((blocks, 2)), dma((blocks, 2, 2)), dma((blocks, 2, 2)),
         ]
         + torus_sems(ny, nz, 2) + torus_sems(nz, ny, 2) + torus_sems(ny, nz, 4) + torus_sems(nz, ny, 4),
         compiler_params=pltpu.CompilerParams(
             collective_id=0, has_side_effects=True, vmem_limit_bytes=56 * 1024 * 1024
         ),
-    )(tokens, *weights, out_a, out_b, gain, mix, sink, cosine, sine)
+    )(tokens, *weights, gain, mix, freq, sink)
 
 
 def local(
@@ -575,22 +582,15 @@
     out_pool_weight,
     out_attn_weight,
 ):
-    rows = tokens.shape[0]
-    positions = lax.axis_index(SP) * rows + jnp.arange(rows, dtype=jnp.int32)
-    cos_r, sin_r, cos_c, sin_c = rope_tables(positions, HD)
-    cosine = jnp.concatenate([cos_r, cos_r, cos_c, cos_c] * 2, 1)
-    sine = jnp.concatenate([-sin_r, sin_r, -sin_c, sin_c] * 2, 1)
-    out_rows = jnp.concatenate([out_pool_weight, out_attn_weight], 0).T
+    lane = np.arange(128)
+    freq = (rope_base ** (-(lane % 16) / 16.0)).astype(np.float32)[None]
     mixed, log_weight = whole_layer(
         tokens,
-        (query_weight, key_weight, value_weight, pool_in_weight),
-        out_rows[:, :384],
-        out_rows[:, 384:],
+        (query_weight, key_weight, value_weight, pool_in_weight, out_pool_weight.T, out_attn_weight.T),
         norm_gain[None],
         pool_mix_weight,
-        jnp.repeat(sink_logit, BLOCK).reshape(2, 4 * BLOCK),
-        cosine,
-        sine,
+        jnp.asarray(freq),
+        sink_logit,
     )
     return (mixed, log_weight)
 

time: 90.4 us -> 77.5 us (0.86)
  Pallas kernels: 80.3 us -> 74.2 us
  local copies, waits for them, and re-layouts: 7.35 us -> 2.48 us
  other arithmetic: 1.93 us -> 0 us
    pallas_call x1, Pallas kernels: 80.3 us -> 74.2 us  [whole_layer(): pl.pallas_call(layer_kernel, out_shape=[jax.ShapeDtypeStruct((rows, width...]
    concatenate x2 -> x0, local copies, waits for them, and re-layouts: 2.85 us -> none  [the longest x1 1.43 us: local(): sine = jnp.concatenate([-sin_r, sin_r, -sin_c, sin_c] * 2, 1)]
    sin x1 -> x0, other arithmetic: 1.9 us -> none  [rope_tables(): jnp.sin(col_angle)]
    unnamed x12 -> x4, local copies, waits for them, and re-layouts: 3.82 us -> 2.48 us
where the time goes in v3:
time: 77.5 us; the launch traced here: 77.3 us
  Pallas kernels  74.2 us (96%)
  local copies, waits for them, and re-layouts  2.48 us (3%)
    pallas_call x1, Pallas kernels, whole_layer(): pl.pallas_call(layer_kernel, out_shape=[jax.ShapeDtypeStruct((rows, width...  74.2 us
    unnamed x4, local copies, waits for them, and re-layouts  2.48 us

profile of v3, /device:TPU:1, one launch (start us, length us, event | category | flops | bytes accessed | tf_op | source)
XLA Modules:
  0.0 77.3 jit_solution(5262355047230542913)
XLA Ops:
  0.6 74.2 %shard_map.122 = (bf16[512,512]{1,0:T(8,128)(2,1)}, f32[8,512]{1,0:T(8,128)}) custom-call(bf16[512,512]{1,0:T(8,128)(2,1)} %tok_ref.1, bf16[16,512]{1,0:T(8,128)(2,1)} %q_ref.1, bf16[16,128]{1,0:T(8,128)(2,1)} %k_ref.1, bf16[16,128]{1,0:T(8,128)(2,1)} %v_ref.1, bf16[16,256]{1,0:T(8,128)(2,1)} %p_ref.1, bf16[16,256]{1,0:T(8,128)(2,1)} %bitcast.4, ...), custom_call_target="tpu_custom_call" | custom-call | tf_op jit(solution)/shard_map/pallas_call | solution.py:536
  74.8 0.0 copy-start
  74.8 1.9 %copy.15 = bf16[512,512]{1,0:T(8,128)(2,1)} copy(bf16[512,512]{1,0:T(8,128)(2,1)} %get-tuple-element.4) | data formatting | bytes 1048576
  76.7 0.0 copy-done
  76.7 0.6 copy.16
Async XLA Ops:
  74.8 1.9 %copy-start = (f32[8,512]{1,0:T(8,128)S(1)}, f32[8,512]{1,0:T(8,128)}, u32[]{:S(2)}) copy-start(f32[8,512]{1,0:T(8,128)} %get-tuple-element.5) | copy-start | bytes 49156

commit v4 on v3

--- a/solution.py
+++ b/solution.py
@@ -78,7 +78,6 @@
         wait_bytes(self.chunk(self.b, 0, count), self.p1_recv.at[self.group_id(k)])
         for way in range(2):
             self.relay(way, k, 1).start()
-        self.to_partner(self.chunk(self.b, self.group_id(k) * self.size, self.size))
 
     def block(self, way, k, back):
         step = 1 if way == 0 else self.n2 - 1
@@ -101,7 +100,12 @@
         wait_bytes(ref, self.p2_recv.at[way, k, hop - 2])
         if hop <= last:
             self.relay(way, k, hop).start()
-        self.to_partner(ref)
+
+    def share(self, back):
+        for way in range(1 if 2 * back in (0, self.n2) else 2):
+            step = 1 if way == 0 else self.n2 - 1
+            origin = lax.rem(self.b + back * (self.n2 - step), self.n2)
+            self.to_partner(self.chunk(origin, 0, self.n1))
 
     def arrived(self):
         wait_bytes(self.buf.at[:, :, 1 - self.c], self.d_recv)
@@ -395,9 +399,9 @@
 
 def layer_kernel(
     tok_ref, q_ref, k_ref, v_ref, p_ref, op_ref, oq_ref,
-    gain_ref, mix_ref, freq_ref, sink_ref,
+    gain_hbm, mix_hbm, freq_ref, sink_ref,
     out_ref, log_ref,
-    t_buf, wa, wb, oa, ob, cos_ref, sin_ref, normed, queries, kv_ext, pool_ext, features,
+    t_buf, wa, wb, oa, ob, gain_ref, mix_ref, cos_ref, sin_ref, normed, queries, kv_ext, pool_ext, features,
     far, near, far_in, near_in, kept,
     load_sem, ring_send, ring_recv, halo_send, halo_recv, far_send, far_recv, near_send, near_recv,
     *torus,
@@ -418,7 +422,11 @@
         pltpu.make_async_copy(oq_ref.at[:, 0:128], oa.at[z, y, c, :, 256:384], load_sem.at[6]),
         pltpu.make_async_copy(oq_ref.at[:, 128:512], ob.at[z, y, c], load_sem.at[7]),
     ]
-    for load in loads:
+    later = [
+        pltpu.make_async_copy(gain_hbm, gain_ref, load_sem.at[8]),
+        pltpu.make_async_copy(mix_hbm, mix_ref, load_sem.at[9]),
+    ]
+    for load in loads + later:
         load.start()
     greet_all()
     for load in loads:
@@ -426,38 +434,25 @@
     for t in ins:
         t.phase1_start()
     ring.start()
+    for load in later:
+        load.wait()
     fill_tables(place, freq_ref, cos_ref, sin_ref)
 
-    def first(group, k):
+    def first(group):
+        for k in range(group[0].groups):
+            for t in group:
+                t.phase1_group(k)
         for t in group:
-            t.phase1_group(k)
+            t.share(0)
 
     def levels(group, hop):
         for k in range(group[0].groups):
             for way in range(2):
                 for t in group:
                     t.level(hop, k, way)
-
-    for k in range(ins[0].groups):
-        first(ins, k)
-    for t in outs:
-        t.phase1_start()
-    levels(ins, 2)
-    ring.forward()
-    levels(ins, 3)
-    for k in range(outs[0].groups):
-        first(outs, k)
-    levels(ins, 4)
-    levels(outs, 2)
-    levels(ins, 5)
-    ring.arrived()
-    levels(outs, 3)
-    normalise(t_buf, gain_ref, normed)
-    for t in ins:
-        t.arrived()
-
-    project_keys(normed, wb, cos_ref, sin_ref, kv_ext)
-    project_pool(normed, wb, pool_ext)
+        for t in group:
+            t.share(hop - 1)
+
 
     def halo_copies(way):
         low = 512 if way == 0 else BLOCK
@@ -476,15 +471,6 @@
             ),
         ]
 
-    for way in range(2):
-        for copy in halo_copies(way):
-            copy.start()
-    for h in range(2):
-        project_queries(normed, wa, cos_ref, sin_ref, queries, h)
-    levels(outs, 4)
-    levels(outs, 5)
-    for t in outs:
-        t.arrived()
     reach = lax.shift_left(jnp.int32(1), x)
     scatter = Scatter(
         (far, near, far_in, near_in, kept), (far_send, far_recv, near_send, near_recv)
@@ -495,6 +481,10 @@
         for h in range(2):
             attend(b, h, place, places, kv_ext, queries, sink_ref, features, log_ref)
         pool(b, place, places, reach, pool_ext, mix_ref, features)
+        return carry
+
+    def send(i, carry):
+        b = lax.rem(i + 1, 4)
         scatter.compute(b, features, oa, ob)
 
         @pl.when(i > 0)
@@ -503,11 +493,43 @@
 
         return carry
 
-    lax.fori_loop(0, 2, block, 0)
+    def both(i, carry):
+        block(i, carry)
+        return send(i, carry)
+
+    for t in outs:
+        t.phase1_start()
+    first(ins)
+    levels(ins, 2)
+    ring.forward()
+    first(outs)
+    levels(ins, 3)
+    levels(outs, 2)
+    levels(ins, 4)
+    levels(outs, 3)
+    ring.arrived()
+    normalise(t_buf, gain_ref, normed)
+    levels(ins, 5)
+    for t in ins:
+        t.arrived()
+    project_keys(normed, wb, cos_ref, sin_ref, kv_ext)
+    project_pool(normed, wb, pool_ext)
+    for way in range(2):
+        for copy in halo_copies(way):
+            copy.start()
+    project_queries(normed, wa, cos_ref, sin_ref, queries, 0)
+    levels(outs, 4)
+    project_queries(normed, wa, cos_ref, sin_ref, queries, 1)
+    block(0, 0)
+    levels(outs, 5)
+    for t in outs:
+        t.arrived()
+    send(0, 0)
+    lax.fori_loop(1, 2, both, 0)
     for way in range(2):
         for copy in halo_copies(way):
             copy.wait_recv()
-    lax.fori_loop(2, 4, block, 0)
+    lax.fori_loop(2, 4, both, 0)
     scatter.add(0)
 
     def close(i, carry):
@@ -539,7 +561,7 @@
             jax.ShapeDtypeStruct((rows, width), bf),
             jax.ShapeDtypeStruct((8, rows), jnp.float32),
         ],
-        in_specs=[pl.BlockSpec(memory_space=pltpu.HBM)] * 7 + [near_data] * 3
+        in_specs=[pl.BlockSpec(memory_space=pltpu.HBM)] * 9 + [near_data]
         + [pl.BlockSpec(memory_space=pltpu.SMEM)],
         out_specs=[near_data] * 2,
         scratch_shapes=[
@@ -548,6 +570,8 @@
             vmem((nz, ny, nc, 16, 512), bf),
             vmem((nz, ny, nc, 16, 384), bf),
             vmem((nz, ny, nc, 16, 384), bf),
+            vmem((1, nx * width), jnp.float32),
+            vmem((1, 256, 256), bf),
             vmem((rows, 128), jnp.float32),
             vmem((rows, 128), jnp.float32),
             vmem((rows, nx * width), bf),
@@ -560,7 +584,7 @@
             vmem((blocks, 2, BLOCK // 2, 512), bf),
             vmem((blocks, 2, BLOCK, 512), bf),
             vmem((blocks, BLOCK, 512), bf),
-            dma((8,)), dma((2, 3)), dma((2, 3)), dma((2, 2)), dma((2, 2)),
+            dma((10,)), dma((2, 3)), dma((2, 3)), dma((2, 2)), dma((2, 2)),
             dma((blocks, 2)), dma((blocks, 2)), dma((blocks, 2, 2)), dma((blocks, 2, 2)),
         ]
         + torus_sems(ny, nz, 2) + torus_sems(nz, ny, 2) + torus_sems(ny, nz, 4) + torus_sems(nz, ny, 4),

time: 77.5 us -> 73.8 us (0.952)
  Pallas kernels: 74.2 us -> 70.6 us
    pallas_call x1, Pallas kernels: 74.2 us -> 70.6 us  [whole_layer(): pl.pallas_call(layer_kernel, out_shape=[jax.ShapeDtypeStruct((rows, width...]
where the time goes in v4:
time: 73.8 us; the launch traced here: 73.7 us
  Pallas kernels  70.6 us (96%)
  local copies, waits for them, and re-layouts  2.48 us (3%)
    pallas_call x1, Pallas kernels, whole_layer(): pl.pallas_call(layer_kernel, out_shape=[jax.ShapeDtypeStruct((rows, width...  70.6 us
    unnamed x4, local copies, waits for them, and re-layouts  2.48 us

profile of v4, /device:TPU:1, one launch (start us, length us, event | category | flops | bytes accessed | tf_op | source)
XLA Modules:
  0.0 73.7 jit_solution(613419969324458734)
XLA Ops:
  0.6 70.6 %shard_map.122 = (bf16[512,512]{1,0:T(8,128)(2,1)}, f32[8,512]{1,0:T(8,128)}) custom-call(bf16[512,512]{1,0:T(8,128)(2,1)} %tok_ref.1, bf16[16,512]{1,0:T(8,128)(2,1)} %q_ref.1, bf16[16,128]{1,0:T(8,128)(2,1)} %k_ref.1, bf16[16,128]{1,0:T(8,128)(2,1)} %v_ref.1, bf16[16,256]{1,0:T(8,128)(2,1)} %p_ref.1, bf16[16,256]{1,0:T(8,128)(2,1)} %bitcast.4, ...), custom_call_target="tpu_custom_call" | custom-call | tf_op jit(solution)/shard_map/pallas_call | solution.py:558
  71.2 0.0 copy-start
  71.2 1.9 %copy.15 = bf16[512,512]{1,0:T(8,128)(2,1)} copy(bf16[512,512]{1,0:T(8,128)(2,1)} %get-tuple-element.4) | data formatting | bytes 1048576
  73.1 0.0 copy-done
  73.1 0.6 copy.16
Async XLA Ops:
  71.2 1.9 %copy-start = (f32[8,512]{1,0:T(8,128)S(1)}, f32[8,512]{1,0:T(8,128)}, u32[]{:S(2)}) copy-start(f32[8,512]{1,0:T(8,128)} %get-tuple-element.5) | copy-start | bytes 49156

commit v5 on v4

--- a/solution.py
+++ b/solution.py
@@ -366,11 +366,11 @@
         across = lax.rem(self.x + 2, self.n)
         self.far[b] = partial_term(b, across, features, oa, ob).astype(jnp.bfloat16)
         for way in range(2):
+            self.far_copy(b, way).start()
+        for way in range(2):
             self.near[b, way] = partial_term(b, self.target(way), features, oa, ob).astype(jnp.bfloat16)
-            self.far_copy(b, way).start()
+            self.near_copy(b, way, False).start()
         self.kept[b] = partial_term(b, self.x, features, oa, ob).astype(jnp.bfloat16)
-        for way in range(2):
-            self.near_copy(b, way, False).start()
 
     def add(self, b):
         for way in range(2):
@@ -378,7 +378,6 @@
             self.far_copy(b, way).wait_recv()
             both = self.near[b, way, rows].astype(jnp.float32) + self.far_in[b, way].astype(jnp.float32)
             self.near[b, way, rows] = both.astype(jnp.bfloat16)
-        for way in range(2):
             self.near_copy(b, way, True).start()
 
     def finish(self, b, out_ref):
@@ -410,7 +409,7 @@
     nz, ny, nc = (lax.axis_size(a) for a in (AX_Z, AX_Y, AX_C))
     place, places = (z * ny + y) * nc + c, nz * ny * nc
     ring = Ring(t_buf, (ring_send, ring_recv))
-    ins = [Torus(wa, AX_Y, 2, torus[0:6]), Torus(wb, AX_Z, 2, torus[6:12])]
+    ins = [Torus(wa, AX_Y, 4, torus[0:6]), Torus(wb, AX_Z, 4, torus[6:12])]
     outs = [Torus(oa, AX_Y, 4, torus[12:18]), Torus(ob, AX_Z, 4, torus[18:24])]
     loads = [
         pltpu.make_async_copy(tok_ref, t_buf.at[x], load_sem.at[0]),
@@ -558,8 +557,8 @@
     return pl.pallas_call(
         layer_kernel,
         out_shape=[
-            jax.ShapeDtypeStruct((rows, width), bf),
-            jax.ShapeDtypeStruct((8, rows), jnp.float32),
+            vmem((rows, width), bf),
+            vmem((8, rows), jnp.float32),
         ],
         in_specs=[pl.BlockSpec(memory_space=pltpu.HBM)] * 9 + [near_data]
         + [pl.BlockSpec(memory_space=pltpu.SMEM)],
@@ -587,7 +586,7 @@
             dma((10,)), dma((2, 3)), dma((2, 3)), dma((2, 2)), dma((2, 2)),
             dma((blocks, 2)), dma((blocks, 2)), dma((blocks, 2, 2)), dma((blocks, 2, 2)),
         ]
-        + torus_sems(ny, nz, 2) + torus_sems(nz, ny, 2) + torus_sems(ny, nz, 4) + torus_sems(nz, ny, 4),
+        + torus_sems(ny, nz, 4) + torus_sems(nz, ny, 4) + torus_sems(ny, nz, 4) + torus_sems(nz, ny, 4),
         compiler_params=pltpu.CompilerParams(
             collective_id=0, has_side_effects=True, vmem_limit_bytes=56 * 1024 * 1024
         ),

time: 73.8 us -> 71.7 us (0.972)
  Pallas kernels: 70.6 us -> 69.5 us
  local copies, waits for them, and re-layouts: 2.48 us -> 1.4 us
    unnamed x4 -> x2, local copies, waits for them, and re-layouts: 2.48 us -> 1.4 us
    pallas_call x1, Pallas kernels: 70.6 us -> 69.5 us  [whole_layer(): pl.pallas_call(layer_kernel, out_shape=[vmem((rows, width), bf), vmem((8,...]
where the time goes in v5:
time: 71.7 us; the launch traced here: 71.6 us
  Pallas kernels  69.5 us (97%)
  local copies, waits for them, and re-layouts  1.4 us (2%)
    pallas_call x1, Pallas kernels, whole_layer(): pl.pallas_call(layer_kernel, out_shape=[vmem((rows, width), bf), vmem((8,...  69.5 us

profile of v5, /device:TPU:1, one launch (start us, length us, event | category | flops | bytes accessed | tf_op | source)
XLA Modules:
  0.0 71.6 jit_solution(11914118825666900810)
XLA Ops:
  0.6 69.5 %shard_map.122 = (bf16[512,512]{1,0:T(8,128)(2,1)S(1)}, f32[8,512]{1,0:T(8,128)S(1)}) custom-call(bf16[512,512]{1,0:T(8,128)(2,1)} %tok_ref.1, bf16[16,512]{1,0:T(8,128)(2,1)} %q_ref.1, bf16[16,128]{1,0:T(8,128)(2,1)} %k_ref.1, bf16[16,128]{1,0:T(8,128)(2,1)} %v_ref.1, bf16[16,256]{1,0:T(8,128)(2,1)} %p_ref.1, bf16[16,256]{1,0:T(8,128)(2,1)} %bitcast.4, ...), custom_call_target="tpu_custom_call" | custom-call | tf_op jit(solution)/shard_map/pallas_call | solution.py:557
  70.2 0.8 %copy.15 = bf16[512,512]{1,0:T(8,128)(2,1)} copy(bf16[512,512]{1,0:T(8,128)(2,1)S(1)} %get-tuple-element.2) | data formatting | bytes 1048576
  71.0 0.6 copy.16

commit v6 on v5

--- a/solution.py
+++ b/solution.py
@@ -410,7 +410,7 @@
     place, places = (z * ny + y) * nc + c, nz * ny * nc
     ring = Ring(t_buf, (ring_send, ring_recv))
     ins = [Torus(wa, AX_Y, 4, torus[0:6]), Torus(wb, AX_Z, 4, torus[6:12])]
-    outs = [Torus(oa, AX_Y, 4, torus[12:18]), Torus(ob, AX_Z, 4, torus[18:24])]
+    outs = [Torus(oa, AX_Y, 8, torus[12:18]), Torus(ob, AX_Z, 8, torus[18:24])]
     loads = [
         pltpu.make_async_copy(tok_ref, t_buf.at[x], load_sem.at[0]),
         pltpu.make_async_copy(q_ref, wa.at[z, y, c], load_sem.at[1]),
@@ -586,7 +586,7 @@
             dma((10,)), dma((2, 3)), dma((2, 3)), dma((2, 2)), dma((2, 2)),
             dma((blocks, 2)), dma((blocks, 2)), dma((blocks, 2, 2)), dma((blocks, 2, 2)),
         ]
-        + torus_sems(ny, nz, 4) + torus_sems(nz, ny, 4) + torus_sems(ny, nz, 4) + torus_sems(nz, ny, 4),
+        + torus_sems(ny, nz, 4) + torus_sems(nz, ny, 4) + torus_sems(ny, nz, 8) + torus_sems(nz, ny, 8),
         compiler_params=pltpu.CompilerParams(
             collective_id=0, has_side_effects=True, vmem_limit_bytes=56 * 1024 * 1024
         ),

time: 71.7 us -> 71 us (level)
  no operation moved by 1% of the time
where the time goes in v6:
time: 71 us; the launch traced here: 70.9 us
  Pallas kernels  68.8 us (97%)
  local copies, waits for them, and re-layouts  1.4 us (2%)
    pallas_call x1, Pallas kernels, whole_layer(): pl.pallas_call(layer_kernel, out_shape=[vmem((rows, width), bf), vmem((8,...  68.8 us

profile of v6, /device:TPU:1, one launch (start us, length us, event | category | flops | bytes accessed | tf_op | source)
XLA Modules:
  0.0 70.9 jit_solution(18429953146833243210)
XLA Ops:
  0.6 68.8 %shard_map.122 = (bf16[512,512]{1,0:T(8,128)(2,1)S(1)}, f32[8,512]{1,0:T(8,128)S(1)}) custom-call(bf16[512,512]{1,0:T(8,128)(2,1)} %tok_ref.1, bf16[16,512]{1,0:T(8,128)(2,1)} %q_ref.1, bf16[16,128]{1,0:T(8,128)(2,1)} %k_ref.1, bf16[16,128]{1,0:T(8,128)(2,1)} %v_ref.1, bf16[16,256]{1,0:T(8,128)(2,1)} %p_ref.1, bf16[16,256]{1,0:T(8,128)(2,1)} %bitcast.4, ...), custom_call_target="tpu_custom_call" | custom-call | tf_op jit(solution)/shard_map/pallas_call | solution.py:557
  69.5 0.8 %copy.15 = bf16[512,512]{1,0:T(8,128)(2,1)} copy(bf16[512,512]{1,0:T(8,128)(2,1)S(1)} %get-tuple-element.2) | data formatting | bytes 1048576
  70.3 0.6 copy.16
